TPU v7x, 32 devices: a whole 2x2x4 slice. The times are simulated.
32 devices in a mesh: fs: 8 (over z, y), tp: 4 (over x, core).
Axes of the slice: x: 2, y: 2, z: 4, core: 2. Of those that a mesh axis runs over, the one named last changes fastest.
Arguments:
- inputs: bfloat16 [4096, 2048], P(('fs', 'tp')), may hold values from -6 to 6
- w_gate: float32 [2048, 5632], P('fs', 'tp'), may hold values from -0.125 to 0.125
- w_value: float32 [2048, 5632], P('fs', 'tp'), may hold values from -0.125 to 0.125
- gate_scale: float32 [5632], P('tp'), may hold values from 0.5 to 2
- value_scale: float32 [5632], P('tp'), may hold values from 0.5 to 2
- conv_gate: float32 [3, 5632], P(None, 'tp'), may hold values from -3.5 to 3.5
- conv_value: float32 [3, 5632], P(None, 'tp'), may hold values from -3.5 to 3.5
- gate_pre: bfloat16 [4096, 5632], P('fs', 'tp'), may hold values from -6 to 6
- value_pre: bfloat16 [4096, 5632], P('fs', 'tp'), may hold values from -6 to 6
- grad_out: bfloat16 [4096, 5632], P('fs', 'tp'), may hold values from -6 to 6
Outputs:
- grad_inputs: bfloat16 [4096, 2048], P(('fs', 'tp'))
- grad_w_gate: float32 [2048, 5632], P('fs', 'tp')
- grad_w_value: float32 [2048, 5632], P('fs', 'tp')
- grad_gate_scale: float32 [5632], P('tp')
- grad_value_scale: float32 [5632], P('tp')
- grad_conv_gate: float32 [3, 5632], P(None, 'tp')
- grad_conv_value: float32 [3, 5632], P(None, 'tp')
All inputs are finite; a program needn't handle non-finite values.
Results may differ from a plain program's by a relative error of at most 0.015.
Values may be sent and summed in bfloat16 or wider, within the bound.
A program may use at most 128 MiB of HBM per device.

v0:
```python
import jax
import jax.numpy as jnp
from jax import lax
from jax.experimental import pallas as pl
from jax.experimental.pallas import tpu as pltpu
from jax.sharding import PartitionSpec as P


BF = jnp.bfloat16
F32 = jnp.float32


LANES = 128


def elementwise(gs_ref, vs_ref, cg_ref, cv_ref, g_ref, v_ref, up_ref, gc_ref, vc_ref, s_ref):
    tokens = g_ref.shape[0]
    row = lax.broadcasted_iota(jnp.int32, g_ref.shape, 0)

    def down(x, k):
        return jnp.where(row >= k, pltpu.roll(x, k, 0), 0.0)

    def up(x, k):
        return jnp.where(row < tokens - k, pltpu.roll(x, tokens - k, 0), 0.0)

    def shifted(ref):
        x = ref[...].astype(F32)
        return down(x, 2), down(x, 1), x

    def conv(taps, xs):
        return taps[0:1] * xs[0] + taps[1:2] * xs[1] + taps[2:3] * xs[2]

    def back(taps, d):
        return (taps[2:3] * d + taps[1:2] * up(d, 1) + taps[0:1] * up(d, 2)).astype(BF)

    gs, vs = shifted(g_ref), shifted(v_ref)
    g = conv(cg_ref[...] * gs_ref[...], gs)
    v = conv(cv_ref[...] * vs_ref[...], vs)
    sig = 1.0 / (1.0 + jnp.exp(-g))
    base = up_ref[...].astype(F32) * sig
    d_gate = base * v * (1.0 + g * (1.0 - sig))
    d_value = base * g
    for j in range(3):
        s_ref[j : j + 1] = jnp.sum(d_gate * gs[j], axis=0, keepdims=True)
        s_ref[3 + j : 4 + j] = jnp.sum(d_value * vs[j], axis=0, keepdims=True)
    s_ref[6:8] = jnp.zeros((2, g_ref.shape[1]), F32)
    gc_ref[...] = back(cg_ref[...], d_gate)
    vc_ref[...] = back(cv_ref[...], d_value)


def cotangents(gs, vs, cg, cv, g, v, up):
    tokens, columns = g.shape
    big = pl.BlockSpec((tokens, LANES), lambda i: (0, i))

    def small(n):
        return pl.BlockSpec((n, LANES), lambda i: (0, i))

    return pl.pallas_call(
        elementwise,
        grid=(pl.cdiv(columns, LANES),),
        in_specs=[small(1), small(1), small(3), small(3), big, big, big],
        out_specs=[big, big, small(8)],
        out_shape=[jax.ShapeDtypeStruct(g.shape, BF)] * 2
        + [jax.ShapeDtypeStruct((8, columns), F32)],
        compiler_params=pltpu.CompilerParams(vmem_limit_bytes=24 * 2**20),
        cost_estimate=pl.CostEstimate(
            flops=g.size * 400, bytes_accessed=g.size * 10, transcendentals=g.size
        ),
    )(gs[None], vs[None], cg, cv, g, v, up)


def rescale(gs_ref, vs_ref, g_ref, v_ref, out_ref):
    out_ref[0] = (g_ref[...] * gs_ref[...]).astype(BF)
    out_ref[1] = (v_ref[...] * vs_ref[...]).astype(BF)


def scaled_weights(gs, vs, g, v):
    own, columns = g.shape
    parts = 4
    block = pl.BlockSpec((own // parts, columns), lambda i: (i, 0))
    scale = pl.BlockSpec((1, columns), lambda i: (0, 0))
    return pl.pallas_call(
        rescale,
        grid=(parts,),
        in_specs=[scale, scale, block, block],
        out_specs=pl.BlockSpec((2, own // parts, columns), lambda i: (0, i, 0)),
        out_shape=jax.ShapeDtypeStruct((2, own, columns), BF),
        compiler_params=pltpu.CompilerParams(vmem_limit_bytes=24 * 2**20),
        cost_estimate=pl.CostEstimate(
            flops=g.size * 100, bytes_accessed=g.size * 12, transcendentals=0
        ),
    )(gs[None], vs[None], g, v)


def tdot(a, b):
    return lax.dot_general(a, b, (((0,), (0,)), ((), ())), preferred_element_type=F32)


def ndot(a, b):
    return lax.dot_general(a, b, (((1,), (1,)), ((), ())), preferred_element_type=F32)


def make(n_fs, n_tp):
    links = n_fs // 2

    def on_device(
        inputs,
        w_gate,
        w_value,
        gate_scale,
        value_scale,
        conv_gate,
        conv_value,
        gate_pre,
        value_pre,
        grad_out,
    ):
        fs = lax.axis_index("fs")
        tp = lax.axis_index("tp")
        c, y = fs // 2, fs % 2
        rows, depth = inputs.shape
        own = w_gate.shape[0]
        half = depth // 2
        tokens, columns = gate_pre.shape

        def swap(x, axis, bit, n):
            return lax.ppermute(x, axis, [(i, i ^ bit) for i in range(n)])

        def chain(x, right, senders):
            step = 1 if right else -1
            pairs = [(2 * s + j, 2 * (s + step) + j) for s in senders for j in (0, 1)]
            return lax.ppermute(x, "fs", pairs)

        stacked = scaled_weights(gate_scale, value_scale, w_gate, w_value)
        rights, lefts = [], []
        r = l = stacked
        for s in range(links - 1):
            r = chain(r, True, range(s, links - 1))
            l = chain(l, False, range(1, links - s))
            rights.append(r)
            lefts.append(l)

        by_half = inputs.reshape(rows, links, 2, own)
        mine = lax.dynamic_index_in_dim(by_half, y, 2, keepdims=False)
        other = lax.dynamic_index_in_dim(by_half, 1 - y, 2, keepdims=False)
        mine, other = mine.reshape(rows, half), other.reshape(rows, half)
        other = swap(other, "fs", 1, n_fs)
        x = jnp.stack([mine, other])[:, None]
        bit = n_tp // 2
        while bit:
            got = swap(x, "tp", bit, n_tp)
            high = (tp // bit) % 2 == 1
            x = jnp.where(high, jnp.stack([got, x], 2), jnp.stack([x, got], 2))
            x = x.reshape(2, -1, rows, half)
            bit //= 2
        x = x.reshape(2, tokens, half)

        gate_cot, value_cot, sums = cotangents(
            gate_scale, value_scale, conv_gate, conv_value, gate_pre, value_pre, grad_out
        )
        bit = 1
        while bit < n_fs:
            sums = sums + swap(sums, "fs", bit, n_fs)
            bit *= 2

        gate_theirs = swap(gate_cot, "fs", 1, n_fs)
        value_theirs = swap(value_cot, "fs", 1, n_fs)
        pair = [(gate_cot, gate_theirs), (value_cot, value_theirs)]

        def at(blocks, i):
            return lax.dynamic_index_in_dim(
                blocks, jnp.clip(i, 0, links - 1), 0, keepdims=False
            )

        def collect(parts):
            r = l = None
            for t in range(links - 1):
                send_r = at(parts, links - 1 - t + c)
                send_l = at(parts, c - (links - 1 - t) + 0)
                if t:
                    send_r = (send_r.astype(F32) + r.astype(F32)).astype(BF)
                    send_l = (send_l.astype(F32) + l.astype(F32)).astype(BF)
                r = chain(send_r, True, range(0, t + 1))
                l = chain(send_l, False, range(links - 1 - t, links))
            total = at(parts, c).astype(F32)
            if r is not None:
                total = total + r.astype(F32) + l.astype(F32)
            return total

        grads = []
        for (cot, theirs), scale in zip(pair, (gate_scale, value_scale)):
            first = tdot(x[0], cot)
            parts = (first + tdot(x[1], theirs)).astype(BF)
            blocks = parts.reshape(links, own, columns)
            grads.append(collect(blocks) * scale)

        blocks = [stacked]
        for s in range(links - 1):
            blocks.append(jnp.where(c > s, rights[s], lefts[links - 2 - s]))
        whole = jnp.concatenate(blocks, 1)
        part = jnp.stack(
            [
                (ndot(g, whole[0]) + ndot(v, whole[1])).astype(BF)
                for g, v in zip(pair[0], pair[1])
            ]
        )
        part = part.reshape(2, n_tp, rows, half)
        bit = 1
        while bit < n_tp:
            split = part.reshape(2, -1, 2, rows, half)
            which = (tp // bit) % 2
            keep = lax.dynamic_index_in_dim(split, which, 2, keepdims=False)
            send = lax.dynamic_index_in_dim(split, 1 - which, 2, keepdims=False)
            got = swap(send, "tp", bit, n_tp)
            part = (keep.astype(F32) + got.astype(F32)).astype(BF)
            bit *= 2
        mine = part.reshape(2, rows, half)[0]
        other = swap(part.reshape(2, rows, half)[1], "fs", 1, n_fs)
        both = jnp.where(
            y == 0, jnp.stack([mine, other], 1), jnp.stack([other, mine], 1)
        ).reshape(rows, 2, links, own)
        order = (c - jnp.arange(links)) % links
        grad_inputs = jnp.take(both, order, axis=2).transpose(0, 2, 1, 3)
        return (
            grad_inputs.reshape(rows, depth),
            grads[0],
            grads[1],
            jnp.sum(conv_gate * sums[0:3], axis=0),
            jnp.sum(conv_value * sums[3:6], axis=0),
            sums[0:3] * gate_scale,
            sums[3:6] * value_scale,
        )

    return on_device


def solution(mesh):
    placed = (
        P(("fs", "tp"), None),
        P("fs", "tp"),
        P("fs", "tp"),
        P("tp"),
        P("tp"),
        P(None, "tp"),
        P(None, "tp"),
        P("fs", "tp"),
        P("fs", "tp"),
        P("fs", "tp"),
    )
    body = make(mesh.shape["fs"], mesh.shape["tp"])

    return jax.shard_map(
        body,
        mesh=mesh,
        in_specs=placed,
        out_specs=(
            P(("fs", "tp"), None),
            P("fs", "tp"),
            P("fs", "tp"),
            P("tp"),
            P("tp"),
            P(None, "tp"),
            P(None, "tp"),
        ),
        check_vma=False,
    )
```

profile of v0, /device:TPU:0, one launch (start us, length us, event | category | flops | bytes accessed | tf_op | source)
XLA Modules:
  0.0 265.6 jit_solution(3541418976828103649)
XLA Ops:
  2.1 3.1 %collective-permute-start.11 = (bf16[128,1024]{0,1:T(8,128)(2,1)S(1)}, bf16[128,1024]{0,1:T(8,128)(2,1)S(1)}, u32[]{:S(2)}, u32[]{:S(2)}) collective-permute-start(bf16[128,1024]{0,1:T(8,128)(2,1)S(1)} %bitcast.114), channel_id=1, source_target_pairs={{0,4},{4,0},{8,12},{12,8},{16,20},{20,16},{24,28},{28,24},{1,5},{5... | collective-permute-start | bytes 786440 | tf_op jit(solution)/shard_map/ppermute | solution.py:127
  5.1 6.3 %collective-permute-done.11 = bf16[128,1024]{0,1:T(8,128)(2,1)S(1)} collective-permute-done((bf16[128,1024]{0,1:T(8,128)(2,1)S(1)}, bf16[128,1024]{0,1:T(8,128)(2,1)S(1)}, u32[]{:S(2)}, u32[]{:S(2)}) %collective-permute-start.11) | collective-permute-done | bytes 262176 | tf_op jit(solution)/shard_map/ppermute | solution.py:127
  15.8 4.8 %collective-permute-start = (bf16[2,256,1408]{2,1,0:T(8,128)(2,1)S(1)}, bf16[2,256,1408]{2,1,0:T(8,128)(2,1)}, u32[]{:S(2)}, u32[]{:S(2)}) collective-permute-start(bf16[2,256,1408]{2,1,0:T(8,128)(2,1)S(1)} %shard_map.154), channel_id=1, source_target_pairs={{0,8},{4,12},{8,16},{12,20},{16,24},{20,28},{1,9},{5,13},{9,17},{1... | collective-permute-start | bytes 4325384 | tf_op jit(solution)/shard_map/ppermute | solution.py:132
  21.9 3.8 %collective-permute-done.12 = bf16[2,1,128,1024]{2,3,0,1:T(8,128)(2,1)} collective-permute-done((bf16[2,1,128,1024]{2,3,0,1:T(8,128)(2,1)}, bf16[2,1,128,1024]{2,3,0,1:T(8,128)(2,1)}, u32[]{:S(2)}, u32[]{:S(2)}) %collective-permute-start.12) | collective-permute-done | bytes 524320 | tf_op jit(solution)/shard_map/ppermute | solution.py:127
  25.7 2.8 %maximum_select_fusion.1 = bf16[2,2,128,1024]{2,3,0,1:T(8,128)(2,1)} fusion(bf16[2,1,128,1024]{2,3,0,1:T(8,128)(2,1)} %get-tuple-element.32, bf16[2,1,128,1024]{2,3,0,1:T(8,128)(2,1)} %collective-permute-done.12, pred[]{:T(512)S(6)} %eq.19), kind=kLoop, calls=%fused_computation.48 | loop fusion | flops 1572864 | bytes 2097153 | tf_op jit(solution)/shard_map/jit(_where)/select_n | solution.py:153
  31.3 8.1 %shard_map.153 = (bf16[512,1408]{1,0:T(8,128)(2,1)}, bf16[512,1408]{1,0:T(8,128)(2,1)S(1)}, f32[8,1408]{1,0:T(8,128)S(1)}) custom-call(f32[1,1408]{1,0:T(1,128)S(1)} %broadcast_in_dim.26.gs_ref, f32[1,1408]{1,0:T(1,128)S(1)} %broadcast_in_dim.27.vs_ref, f32[3,1408]{1,0:T(4,128)S(1)} %copy-done.7, f32[3,1408]{1,0:T(4,128)S(1)} %copy-done.8, ...), custom_call_target="tpu_custom_call" | custom-call | flops 288358400 | bytes 7208960 | tf_op jit(solution)/shard_map/pallas_call | solution.py:58
  42.6 33.1 %collective-permute-done.26 = f32[8,1408]{1,0:T(8,128)S(1)} collective-permute-done((f32[8,1408]{1,0:T(8,128)S(1)}, f32[8,1408]{1,0:T(8,128)S(1)}, u32[]{:S(2)}, u32[]{:S(2)}) %collective-permute-start.26) | collective-permute-done | bytes 45088 | tf_op jit(solution)/shard_map/ppermute | solution.py:127
  80.8 1.8 collective-permute-start.4
  83.8 1.9 maximum_select_fusion
  88.8 6.1 %fusion.28 = f32[1024,1408]{1,0:T(8,128)} fusion(bf16[512,1024]{1,0:T(8,128)(2,1)S(1)} %bitcast.106, bf16[512,1408]{1,0:T(8,128)(2,1)} %get-tuple-element.10), kind=kOutput, calls=%fused_computation.83 | convolution fusion | flops 1476395008 | bytes 8257536 | tf_op jit(solution)/shard_map/dot_general | solution.py:96
  96.4 5.3 %add_convert_fusion.1 = bf16[1024,1408]{1,0:T(8,128)(2,1)S(1)} fusion(f32[1024,1408]{1,0:T(8,128)} %fusion.28, bf16[512,1024]{1,0:T(8,128)(2,1)S(1)} %bitcast.104, bf16[512,1408]{1,0:T(8,128)(2,1)} %collective-permute-done.6), kind=kOutput, calls=%fused_computation.3 | convolution fusion | flops 1479278592 | bytes 11141120 | tf_op jit(solution)/shard_map/dot_general | solution.py:96
  103.9 7.9 %collective-permute-start.14 = (bf16[256,1408]{1,0:T(8,128)(2,1)}, bf16[256,1408]{1,0:T(8,128)(2,1)}, u32[]{:S(2)}, u32[]{:S(2)}) collective-permute-start(bf16[256,1408]{1,0:T(8,128)(2,1)} %get-tuple-element.28), channel_id=1, source_target_pairs={{0,8},{4,12},{1,9},{5,13},{2,10},{6,14},{3,11},{7,15}} | collective-permute-start | bytes 2162696 | tf_op jit(solution)/shard_map/ppermute | solution.py:132
  111.8 1.9 fusion.29
  113.7 3.2 %add_convert_fusion = bf16[1024,1408]{1,0:T(8,128)(2,1)S(1)} fusion(f32[1024,1408]{1,0:T(8,128)S(1)} %fusion.29, bf16[512,1024]{1,0:T(8,128)(2,1)S(1)} %bitcast.105, bf16[512,1408]{1,0:T(8,128)(2,1)} %collective-permute-done.7), kind=kOutput, calls=%fused_computation.2 | convolution fusion | flops 1479278592 | bytes 11141120 | tf_op jit(solution)/shard_map/dot_general | solution.py:96
  118.9 2.2 collective-permute-start.20
  122.7 19.3 %collective-permute-done.28 = f32[8,1408]{1,0:T(8,128)S(1)} collective-permute-done((f32[8,1408]{1,0:T(8,128)S(1)}, f32[8,1408]{1,0:T(8,128)S(1)}, u32[]{:S(2)}, u32[]{:S(2)}) %collective-permute-start.28) | collective-permute-done | bytes 45088 | tf_op jit(solution)/shard_map/ppermute | solution.py:127
  147.8 7.9 %collective-permute-start.21 = (bf16[256,1408]{1,0:T(8,128)(2,1)S(1)}, bf16[256,1408]{1,0:T(8,128)(2,1)S(1)}, u32[]{:S(2)}, u32[]{:S(2)}) collective-permute-start(bf16[256,1408]{1,0:T(8,128)(2,1)S(1)} %fusion.7), channel_id=1, source_target_pairs={{0,8},{4,12},{8,16},{12,20},{1,9},{5,13},{9,17},{13,21},{2,10},{6,... | collective-permute-start | bytes 2162696 | tf_op jit(solution)/shard_map/ppermute | solution.py:132
  159.8 3.0 %collective-permute-done.15 = bf16[256,1408]{1,0:T(8,128)(2,1)S(1)} collective-permute-done((bf16[256,1408]{1,0:T(8,128)(2,1)S(1)}, bf16[256,1408]{1,0:T(8,128)(2,1)S(1)}, u32[]{:S(2)}, u32[]{:S(2)}) %collective-permute-start.15) | collective-permute-done | bytes 720928 | tf_op jit(solution)/shard_map/ppermute | solution.py:132
  165.7 9.8 %collective-permute-done.21 = bf16[256,1408]{1,0:T(8,128)(2,1)S(1)} collective-permute-done((bf16[256,1408]{1,0:T(8,128)(2,1)S(1)}, bf16[256,1408]{1,0:T(8,128)(2,1)S(1)}, u32[]{:S(2)}, u32[]{:S(2)}) %collective-permute-start.21) | collective-permute-done | bytes 720928 | tf_op jit(solution)/shard_map/ppermute | solution.py:132
  180.1 11.1 %collective-permute-done.3 = bf16[2,256,1408]{2,1,0:T(8,128)(2,1)S(1)} collective-permute-done((bf16[2,256,1408]{2,1,0:T(8,128)(2,1)}, bf16[2,256,1408]{2,1,0:T(8,128)(2,1)S(1)}, u32[]{:S(2)}, u32[]{:S(2)}) %collective-permute-start.3) | collective-permute-done | bytes 1441824 | tf_op jit(solution)/shard_map/ppermute | solution.py:132
  191.5 7.8 %pad_maximum_fusion = bf16[2,1024,1408]{2,1,0:T(8,128)(2,1)S(1)} fusion(bf16[2,256,1408]{2,1,0:T(8,128)(2,1)S(1)} %broadcast_select_fusion, bf16[2,256,1408]{2,1,0:T(8,128)(2,1)S(1)} %broadcast_select_fusion.1, bf16[2,256,1408]{2,1,0:T(8,128)(2,1)S(1)} %broadcast_select_fusion.2, bf16[2,256,1408]{2,1,0:T(8,128)(2,1)S(1)} %shard_map.154), kind=kLoop, calls=%fused_computation.1 | loop fusion | flops 23068672 | bytes 11534336 | tf_op jit(solution)/shard_map/concatenate | solution.py:200
  199.3 1.8 fusion.3
  201.8 3.2 %add_convert_fusion.3 = bf16[512,1024]{1,0:T(8,128)(2,1)S(1)} fusion(f32[512,1024]{1,0:T(8,128)S(1)} %fusion.3, bf16[512,1408]{1,0:T(8,128)(2,1)} %get-tuple-element.10, bf16[2,1024,1408]{2,1,0:T(8,128)(2,1)S(1)} %pad_maximum_fusion), kind=kOutput, calls=%fused_computation.18 | convolution fusion | flops 1477443584 | bytes 7471104 | tf_op jit(solution)/shard_map/dot_general | solution.py:100
  206.3 4.2 %fusion.2 = f32[512,1024]{1,0:T(8,128)S(1)} fusion(bf16[512,1408]{1,0:T(8,128)(2,1)} %collective-permute-done.7, bf16[2,1024,1408]{2,1,0:T(8,128)(2,1)} %copy-done.21), kind=kOutput, calls=%fused_computation.8 | convolution fusion | flops 1476395008 | bytes 6422528 | tf_op jit(solution)/shard_map/dot_general | solution.py:100
  210.5 4.2 %add_convert_fusion.2 = bf16[512,1024]{1,0:T(8,128)(2,1)} fusion(f32[512,1024]{1,0:T(8,128)S(1)} %fusion.2, bf16[512,1408]{1,0:T(8,128)(2,1)} %collective-permute-done.6, bf16[2,1024,1408]{2,1,0:T(8,128)(2,1)S(1)} %copy-done.22), kind=kOutput, calls=%fused_computation.17 | convolution fusion | flops 1477443584 | bytes 7471104 | tf_op jit(solution)/shard_map/dot_general | solution.py:100
  214.7 2.4 copy.18
  219.9 2.9 %collective-permute-start.16 = (bf16[256,1408]{1,0:T(8,128)(2,1)}, bf16[256,1408]{1,0:T(8,128)(2,1)S(1)}, u32[]{:S(2)}, u32[]{:S(2)}) collective-permute-start(bf16[256,1408]{1,0:T(8,128)(2,1)} %get-tuple-element.26), channel_id=1, source_target_pairs={{0,8},{4,12},{8,16},{12,20},{16,24},{20,28},{1,9},{5,13},{9,17},{1... | collective-permute-start | bytes 2162696 | tf_op jit(solution)/shard_map/ppermute | solution.py:132
  222.9 1.9 collective-permute-start.22
  232.1 7.5 %collective-permute-done.16 = bf16[256,1408]{1,0:T(8,128)(2,1)S(1)} collective-permute-done((bf16[256,1408]{1,0:T(8,128)(2,1)}, bf16[256,1408]{1,0:T(8,128)(2,1)S(1)}, u32[]{:S(2)}, u32[]{:S(2)}) %collective-permute-start.16) | collective-permute-done | bytes 720928 | tf_op jit(solution)/shard_map/ppermute | solution.py:132
  239.6 7.5 %collective-permute-done.19 = bf16[256,1408]{1,0:T(8,128)(2,1)S(1)} collective-permute-done((bf16[256,1408]{1,0:T(8,128)(2,1)S(1)}, bf16[256,1408]{1,0:T(8,128)(2,1)S(1)}, u32[]{:S(2)}, u32[]{:S(2)}) %collective-permute-start.19) | collective-permute-done | bytes 720928 | tf_op jit(solution)/shard_map/ppermute | solution.py:132
  249.3 5.3 %collective-permute-done.22 = bf16[256,1408]{1,0:T(8,128)(2,1)S(1)} collective-permute-done((bf16[256,1408]{1,0:T(8,128)(2,1)}, bf16[256,1408]{1,0:T(8,128)(2,1)S(1)}, u32[]{:S(2)}, u32[]{:S(2)}) %collective-permute-start.22) | collective-permute-done | bytes 720928 | tf_op jit(solution)/shard_map/ppermute | solution.py:132
  254.6 7.2 %collective-permute-done.25 = bf16[256,1408]{1,0:T(8,128)(2,1)S(1)} collective-permute-done((bf16[256,1408]{1,0:T(8,128)(2,1)S(1)}, bf16[256,1408]{1,0:T(8,128)(2,1)S(1)}, u32[]{:S(2)}, u32[]{:S(2)}) %collective-permute-start.25) | collective-permute-done | bytes 720928 | tf_op jit(solution)/shard_map/ppermute | solution.py:132
  (132 shorter events, 64.8 us)
Async XLA Ops:
  2.1 9.4 %collective-permute-start.11 = (bf16[128,1024]{0,1:T(8,128)(2,1)S(1)}, bf16[128,1024]{0,1:T(8,128)(2,1)S(1)}, u32[]{:S(2)}, u32[]{:S(2)}) collective-permute-start(bf16[128,1024]{0,1:T(8,128)(2,1)S(1)} %bitcast.114), channel_id=1, source_target_pairs={{0,4},{4,0},{8,12},{12,8},{16,20},{20,16},{24,28},{28,24},{1,5},{5... | collective-permute-start | bytes 786440 | tf_op jit(solution)/shard_map/ppermute | solution.py:127
  12.3 13.4 %collective-permute-start.12 = (bf16[2,1,128,1024]{2,3,0,1:T(8,128)(2,1)}, bf16[2,1,128,1024]{2,3,0,1:T(8,128)(2,1)}, u32[]{:S(2)}, u32[]{:S(2)}) collective-permute-start(bf16[2,1,128,1024]{2,3,0,1:T(8,128)(2,1)} %get-tuple-element.32), channel_id=1, source_target_pairs={{0,2},{1,3},{2,0},{3,1},{4,6},{5,7},{6,4},{7,5},{8,10},{9,11},{10,... | collective-permute-start | bytes 1572872 | tf_op jit(solution)/shard_map/ppermute | solution.py:127
  15.7 12.8 %copy-start.2 = (bf16[512,1408]{1,0:T(8,128)(2,1)S(1)}, bf16[512,1408]{1,0:T(8,128)(2,1)}, u32[]{:S(2)}) copy-start(bf16[512,1408]{1,0:T(8,128)(2,1)} %g_ref.2) | copy-start | bytes 4325380
  15.8 63.4 %collective-permute-start = (bf16[2,256,1408]{2,1,0:T(8,128)(2,1)S(1)}, bf16[2,256,1408]{2,1,0:T(8,128)(2,1)}, u32[]{:S(2)}, u32[]{:S(2)}) collective-permute-start(bf16[2,256,1408]{2,1,0:T(8,128)(2,1)S(1)} %shard_map.154), channel_id=1, source_target_pairs={{0,8},{4,12},{8,16},{12,20},{16,24},{20,28},{1,9},{5,13},{9,17},{1... | collective-permute-start | bytes 4325384 | tf_op jit(solution)/shard_map/ppermute | solution.py:132
  20.6 60.2 %collective-permute-start.1 = (bf16[2,256,1408]{2,1,0:T(8,128)(2,1)S(1)}, bf16[2,256,1408]{2,1,0:T(8,128)(2,1)}, u32[]{:S(2)}, u32[]{:S(2)}) collective-permute-start(bf16[2,256,1408]{2,1,0:T(8,128)(2,1)S(1)} %shard_map.154), channel_id=1, source_target_pairs={{8,0},{12,4},{16,8},{20,12},{24,16},{28,20},{9,1},{13,5},{17,9},{2... | collective-permute-start | bytes 4325384 | tf_op jit(solution)/shard_map/ppermute | solution.py:132
  28.5 54.0 %collective-permute-start.13 = (bf16[2,2,128,1024]{2,3,0,1:T(8,128)(2,1)}, bf16[2,2,128,1024]{2,3,0,1:T(8,128)(2,1)}, u32[]{:S(2)}, u32[]{:S(2)}) collective-permute-start(bf16[2,2,128,1024]{2,3,0,1:T(8,128)(2,1)} %maximum_select_fusion.1), channel_id=1, source_target_pairs={{0,1},{1,0},{2,3},{3,2},{4,5},{5,4},{6,7},{7,6},{8,9},{9,8},{10,11... | collective-permute-start | bytes 3145736 | tf_op jit(solution)/shard_map/ppermute | solution.py:127
  40.5 55.9 %collective-permute-start.6 = (bf16[512,1408]{1,0:T(8,128)(2,1)}, bf16[512,1408]{1,0:T(8,128)(2,1)}, u32[]{:S(2)}, u32[]{:S(2)}) collective-permute-start(bf16[512,1408]{1,0:T(8,128)(2,1)} %get-tuple-element.10), channel_id=1, source_target_pairs={{0,4},{4,0},{8,12},{12,8},{16,20},{20,16},{24,28},{28,24},{1,5},{5... | collective-permute-start | bytes 4325384 | tf_op jit(solution)/shard_map/ppermute | solution.py:127
  42.0 33.7 %collective-permute-start.26 = (f32[8,1408]{1,0:T(8,128)S(1)}, f32[8,1408]{1,0:T(8,128)S(1)}, u32[]{:S(2)}, u32[]{:S(2)}) collective-permute-start(f32[8,1408]{1,0:T(8,128)S(1)} %get-tuple-element.12), channel_id=1, source_target_pairs={{0,4},{4,0},{8,12},{12,8},{16,20},{20,16},{24,28},{28,24},{1,5},{5... | collective-permute-start | bytes 135176 | tf_op jit(solution)/shard_map/ppermute | solution.py:127
  75.7 38.0 %collective-permute-start.7 = (bf16[512,1408]{1,0:T(8,128)(2,1)}, bf16[512,1408]{1,0:T(8,128)(2,1)}, u32[]{:S(2)}, u32[]{:S(2)}) collective-permute-start(bf16[512,1408]{1,0:T(8,128)(2,1)} %copy-done.5), channel_id=1, source_target_pairs={{0,4},{4,0},{8,12},{12,8},{16,20},{20,16},{24,28},{28,24},{1,5},{5... | collective-permute-start | bytes 4325384 | tf_op jit(solution)/shard_map/ppermute | solution.py:127
  79.1 42.0 %collective-permute-start.27 = (f32[8,1408]{1,0:T(8,128)}, f32[8,1408]{1,0:T(8,128)S(1)}, u32[]{:S(2)}, u32[]{:S(2)}) collective-permute-start(f32[8,1408]{1,0:T(8,128)} %add.198), channel_id=1, source_target_pairs={{0,8},{4,12},{8,0},{12,4},{16,24},{20,28},{24,16},{28,20},{1,9},{5... | collective-permute-start | bytes 135176 | tf_op jit(solution)/shard_map/ppermute | solution.py:127
  80.8 67.0 %collective-permute-start.4 = (bf16[2,256,1408]{2,1,0:T(8,128)(2,1)}, bf16[2,256,1408]{2,1,0:T(8,128)(2,1)}, u32[]{:S(2)}, u32[]{:S(2)}) collective-permute-start(bf16[2,256,1408]{2,1,0:T(8,128)(2,1)} %collective-permute-done), channel_id=1, source_target_pairs={{8,16},{12,20},{16,24},{20,28},{9,17},{13,21},{17,25},{21,29},{10,... | collective-permute-start | bytes 4325384 | tf_op jit(solution)/shard_map/ppermute | solution.py:132
  82.6 73.2 %collective-permute-start.2 = (bf16[2,256,1408]{2,1,0:T(8,128)(2,1)}, bf16[2,256,1408]{2,1,0:T(8,128)(2,1)}, u32[]{:S(2)}, u32[]{:S(2)}) collective-permute-start(bf16[2,256,1408]{2,1,0:T(8,128)(2,1)} %collective-permute-done.1), channel_id=1, source_target_pairs={{8,0},{12,4},{16,8},{20,12},{9,1},{13,5},{17,9},{21,13},{10,2},{14... | collective-permute-start | bytes 4325384 | tf_op jit(solution)/shard_map/ppermute | solution.py:132
  103.9 38.8 %collective-permute-start.14 = (bf16[256,1408]{1,0:T(8,128)(2,1)}, bf16[256,1408]{1,0:T(8,128)(2,1)}, u32[]{:S(2)}, u32[]{:S(2)}) collective-permute-start(bf16[256,1408]{1,0:T(8,128)(2,1)} %get-tuple-element.28), channel_id=1, source_target_pairs={{0,8},{4,12},{1,9},{5,13},{2,10},{6,14},{3,11},{7,15}} | collective-permute-start | bytes 2162696 | tf_op jit(solution)/shard_map/ppermute | solution.py:132
  118.9 26.0 %collective-permute-start.20 = (bf16[256,1408]{1,0:T(8,128)(2,1)}, bf16[256,1408]{1,0:T(8,128)(2,1)}, u32[]{:S(2)}, u32[]{:S(2)}) collective-permute-start(bf16[256,1408]{1,0:T(8,128)(2,1)} %get-tuple-element.24), channel_id=1, source_target_pairs={{0,8},{4,12},{1,9},{5,13},{2,10},{6,14},{3,11},{7,15}} | collective-permute-start | bytes 2162696 | tf_op jit(solution)/shard_map/ppermute | solution.py:132
  121.9 20.1 %collective-permute-start.28 = (f32[8,1408]{1,0:T(8,128)S(1)}, f32[8,1408]{1,0:T(8,128)S(1)}, u32[]{:S(2)}, u32[]{:S(2)}) collective-permute-start(f32[8,1408]{1,0:T(8,128)S(1)} %add.199), channel_id=1, source_target_pairs={{0,16},{4,20},{8,24},{12,28},{16,0},{20,4},{24,8},{28,12},{1,17},{... | collective-permute-start | bytes 135176 | tf_op jit(solution)/shard_map/ppermute | solution.py:127
  142.0 16.2 %collective-permute-start.17 = (bf16[256,1408]{1,0:T(8,128)(2,1)}, bf16[256,1408]{1,0:T(8,128)(2,1)S(1)}, u32[]{:S(2)}, u32[]{:S(2)}) collective-permute-start(bf16[256,1408]{1,0:T(8,128)(2,1)} %get-tuple-element.29), channel_id=1, source_target_pairs={{24,16},{28,20},{25,17},{29,21},{26,18},{30,22},{27,19},{31,23}} | collective-permute-start | bytes 2162696 | tf_op jit(solution)/shard_map/ppermute | solution.py:132
  142.7 23.0 %collective-permute-start.23 = (bf16[256,1408]{1,0:T(8,128)(2,1)}, bf16[256,1408]{1,0:T(8,128)(2,1)S(1)}, u32[]{:S(2)}, u32[]{:S(2)}) collective-permute-start(bf16[256,1408]{1,0:T(8,128)(2,1)} %get-tuple-element.25), channel_id=1, source_target_pairs={{24,16},{28,20},{25,17},{29,21},{26,18},{30,22},{27,19},{31,23}} | collective-permute-start | bytes 2162696 | tf_op jit(solution)/shard_map/ppermute | solution.py:132
  144.9 17.8 %collective-permute-start.15 = (bf16[256,1408]{1,0:T(8,128)(2,1)S(1)}, bf16[256,1408]{1,0:T(8,128)(2,1)S(1)}, u32[]{:S(2)}, u32[]{:S(2)}) collective-permute-start(bf16[256,1408]{1,0:T(8,128)(2,1)S(1)} %fusion.13), channel_id=1, source_target_pairs={{0,8},{4,12},{8,16},{12,20},{1,9},{5,13},{9,17},{13,21},{2,10},{6,... | collective-permute-start | bytes 2162696 | tf_op jit(solution)/shard_map/ppermute | solution.py:132
  147.8 15.0 %copy-start.13 = (bf16[1024,1408]{1,0:T(8,128)(2,1)S(1)}, bf16[1024,1408]{1,0:T(8,128)(2,1)}, u32[]{:S(2)}) copy-start(bf16[1024,1408]{1,0:T(8,128)(2,1)} %copy-done.12) | copy-start | bytes 8650756
  147.8 27.7 %collective-permute-start.21 = (bf16[256,1408]{1,0:T(8,128)(2,1)S(1)}, bf16[256,1408]{1,0:T(8,128)(2,1)S(1)}, u32[]{:S(2)}, u32[]{:S(2)}) collective-permute-start(bf16[256,1408]{1,0:T(8,128)(2,1)S(1)} %fusion.7), channel_id=1, source_target_pairs={{0,8},{4,12},{8,16},{12,20},{1,9},{5,13},{9,17},{13,21},{2,10},{6,... | collective-permute-start | bytes 2162696 | tf_op jit(solution)/shard_map/ppermute | solution.py:132
  155.7 22.8 %collective-permute-start.5 = (bf16[2,256,1408]{2,1,0:T(8,128)(2,1)}, bf16[2,256,1408]{2,1,0:T(8,128)(2,1)S(1)}, u32[]{:S(2)}, u32[]{:S(2)}) collective-permute-start(bf16[2,256,1408]{2,1,0:T(8,128)(2,1)} %collective-permute-done.4), channel_id=1, source_target_pairs={{16,24},{20,28},{17,25},{21,29},{18,26},{22,30},{19,27},{23,31}} | collective-permute-start | bytes 4325384 | tf_op jit(solution)/shard_map/ppermute | solution.py:132
  158.2 17.3 %copy-start.10 = (bf16[1024,1408]{1,0:T(8,128)(2,1)S(1)}, bf16[1024,1408]{1,0:T(8,128)(2,1)}, u32[]{:S(2)}) copy-start(bf16[1024,1408]{1,0:T(8,128)(2,1)} %copy-done.9) | copy-start | bytes 8650756
  158.2 33.0 %collective-permute-start.3 = (bf16[2,256,1408]{2,1,0:T(8,128)(2,1)}, bf16[2,256,1408]{2,1,0:T(8,128)(2,1)S(1)}, u32[]{:S(2)}, u32[]{:S(2)}) collective-permute-start(bf16[2,256,1408]{2,1,0:T(8,128)(2,1)} %collective-permute-done.2), channel_id=1, source_target_pairs={{8,0},{12,4},{9,1},{13,5},{10,2},{14,6},{11,3},{15,7}} | collective-permute-start | bytes 4325384 | tf_op jit(solution)/shard_map/ppermute | solution.py:132
  164.2 60.6 %collective-permute-start.18 = (bf16[256,1408]{1,0:T(8,128)(2,1)}, bf16[256,1408]{1,0:T(8,128)(2,1)}, u32[]{:S(2)}, u32[]{:S(2)}) collective-permute-start(bf16[256,1408]{1,0:T(8,128)(2,1)} %get-tuple-element.27), channel_id=1, source_target_pairs={{16,8},{20,12},{24,16},{28,20},{17,9},{21,13},{25,17},{29,21},{18,... | collective-permute-start | bytes 2162696 | tf_op jit(solution)/shard_map/ppermute | solution.py:132
  177.0 50.6 %collective-permute-start.24 = (bf16[256,1408]{1,0:T(8,128)(2,1)}, bf16[256,1408]{1,0:T(8,128)(2,1)}, u32[]{:S(2)}, u32[]{:S(2)}) collective-permute-start(bf16[256,1408]{1,0:T(8,128)(2,1)} %get-tuple-element.23), channel_id=1, source_target_pairs={{16,8},{20,12},{24,16},{28,20},{17,9},{21,13},{25,17},{29,21},{18,... | collective-permute-start | bytes 2162696 | tf_op jit(solution)/shard_map/ppermute | solution.py:132
  218.6 11.6 %collective-permute-start.8 = (bf16[2,2,128,1024]{2,3,1,0:T(8,128)(2,1)S(1)}, bf16[2,2,128,1024]{2,3,1,0:T(8,128)(2,1)S(1)}, u32[]{:S(2)}, u32[]{:S(2)}) collective-permute-start(bf16[2,2,128,1024]{2,3,1,0:T(8,128)(2,1)S(1)} %fusion.18), channel_id=1, source_target_pairs={{0,1},{1,0},{2,3},{3,2},{4,5},{5,4},{6,7},{7,6},{8,9},{9,8},{10,11... | collective-permute-start | bytes 3145736 | tf_op jit(solution)/shard_map/ppermute | solution.py:127
  219.9 19.7 %collective-permute-start.16 = (bf16[256,1408]{1,0:T(8,128)(2,1)}, bf16[256,1408]{1,0:T(8,128)(2,1)S(1)}, u32[]{:S(2)}, u32[]{:S(2)}) collective-permute-start(bf16[256,1408]{1,0:T(8,128)(2,1)} %get-tuple-element.26), channel_id=1, source_target_pairs={{0,8},{4,12},{8,16},{12,20},{16,24},{20,28},{1,9},{5,13},{9,17},{1... | collective-permute-start | bytes 2162696 | tf_op jit(solution)/shard_map/ppermute | solution.py:132
  222.9 31.8 %collective-permute-start.22 = (bf16[256,1408]{1,0:T(8,128)(2,1)}, bf16[256,1408]{1,0:T(8,128)(2,1)S(1)}, u32[]{:S(2)}, u32[]{:S(2)}) collective-permute-start(bf16[256,1408]{1,0:T(8,128)(2,1)} %get-tuple-element.22), channel_id=1, source_target_pairs={{0,8},{4,12},{8,16},{12,20},{16,24},{20,28},{1,9},{5,13},{9,17},{1... | collective-permute-start | bytes 2162696 | tf_op jit(solution)/shard_map/ppermute | solution.py:132
  226.1 21.0 %collective-permute-start.19 = (bf16[256,1408]{1,0:T(8,128)(2,1)S(1)}, bf16[256,1408]{1,0:T(8,128)(2,1)S(1)}, u32[]{:S(2)}, u32[]{:S(2)}) collective-permute-start(bf16[256,1408]{1,0:T(8,128)(2,1)S(1)} %fusion.12), channel_id=1, source_target_pairs={{8,0},{12,4},{16,8},{20,12},{24,16},{28,20},{9,1},{13,5},{17,9},{2... | collective-permute-start | bytes 2162696 | tf_op jit(solution)/shard_map/ppermute | solution.py:132
  228.9 33.0 %collective-permute-start.25 = (bf16[256,1408]{1,0:T(8,128)(2,1)S(1)}, bf16[256,1408]{1,0:T(8,128)(2,1)S(1)}, u32[]{:S(2)}, u32[]{:S(2)}) collective-permute-start(bf16[256,1408]{1,0:T(8,128)(2,1)S(1)} %fusion.6), channel_id=1, source_target_pairs={{8,0},{12,4},{16,8},{20,12},{24,16},{28,20},{9,1},{13,5},{17,9},{2... | collective-permute-start | bytes 2162696 | tf_op jit(solution)/shard_map/ppermute | solution.py:132
  230.6 18.0 %collective-permute-start.9 = (bf16[2,1,128,1024]{2,3,1,0:T(8,128)(2,1)S(1)}, bf16[2,1,128,1024]{2,3,1,0:T(8,128)(2,1)S(1)}, u32[]{:S(2)}, u32[]{:S(2)}) collective-permute-start(bf16[2,1,128,1024]{2,3,1,0:T(8,128)(2,1)S(1)} %constant_dynamic-slice_fusion.2), channel_id=1, source_target_pairs={{0,2},{1,3},{2,0},{3,1},{4,6},{5,7},{6,4},{7,5},{8,10},{9,11},{10,... | collective-permute-start | bytes 1572872 | tf_op jit(solution)/shard_map/ppermute | solution.py:127
  248.7 14.7 %collective-permute-start.10 = (bf16[128,1024]{0,1:T(8,128)(2,1)S(1)}, bf16[128,1024]{0,1:T(8,128)(2,1)S(1)}, u32[]{:S(2)}, u32[]{:S(2)}) collective-permute-start(bf16[128,1024]{0,1:T(8,128)(2,1)S(1)} %get-tuple-element.37), channel_id=1, source_target_pairs={{0,4},{4,0},{8,12},{12,8},{16,20},{20,16},{24,28},{28,24},{1,5},{5... | collective-permute-start | bytes 786440 | tf_op jit(solution)/shard_map/ppermute | solution.py:127
  (22 other events, 148.0 us)
where the time goes:
time: 267 us; the launch traced here: 266 us
  waiting for transfers between devices  114 us (43%)
  starting transfers between devices  55.9 us (21%)
  other arithmetic  34.1 us (13%)
  matrix products  29.8 us (11%)
  local copies, waits for them, and re-layouts  21.9 us (8%)
  Pallas kernels  8.45 us (3%)
    ppermute x11, waiting for transfers between devices, swap(): return lax.ppermute(x, axis, [(i, i ^ bit) for i in range(n)])  62.5 us
    ppermute x18, waiting for transfers between devices, chain(): return lax.ppermute(x, 'fs', pairs)  51.5 us
    ppermute x18, starting transfers between devices, chain(): return lax.ppermute(x, 'fs', pairs)  43.1 us
    dot_general x4, matrix products, tdot(): lax.dot_general(a, b, (((0,), (0,)), ((), ())), preferred_element_type=F32)  16.4 us
    dot_general x4, matrix products, ndot(): lax.dot_general(a, b, (((1,), (1,)), ((), ())), preferred_element_type=F32)  13.4 us
    ppermute x11, starting transfers between devices, swap(): return lax.ppermute(x, axis, [(i, i ^ bit) for i in range(n)])  12.8 us
    unnamed x52, local copies, waits for them, and re-layouts  9.82 us
    pallas_call x1, Pallas kernels, cotangents(): pl.pallas_call(elementwise, grid=(pl.cdiv(columns, LANES),), in_specs=[sm...  8.13 us
  transfers between devices with their start and end apart: 29, of which 11 were waited for; matrix products, arithmetic and copies ran while one was open for 28% of the time, Pallas kernels for 3%

commit v1 on v0

--- a/solution.py
+++ b/solution.py
@@ -197,13 +197,15 @@
         blocks = [stacked]
         for s in range(links - 1):
             blocks.append(jnp.where(c > s, rights[s], lefts[links - 2 - s]))
-        whole = jnp.concatenate(blocks, 1)
-        part = jnp.stack(
-            [
-                (ndot(g, whole[0]) + ndot(v, whole[1])).astype(BF)
-                for g, v in zip(pair[0], pair[1])
-            ]
-        )
+        columns_of = []
+        for block in blocks:
+            columns_of.append(
+                [
+                    (ndot(g, block[0]) + ndot(v, block[1])).astype(BF)
+                    for g, v in zip(pair[0], pair[1])
+                ]
+            )
+        part = jnp.stack([jnp.concatenate(t, 1) for t in zip(*columns_of)])
         part = part.reshape(2, n_tp, rows, half)
         bit = 1
         while bit < n_tp:

time: 267 us -> 246 us (0.921)
  waiting for transfers between devices: 114 us -> 96 us
  matrix products: 29.8 us -> 41.8 us
  other arithmetic: 34.1 us -> 24.3 us
  starting transfers between devices: 55.9 us -> 49.5 us
    ppermute x11, waiting for transfers between devices: 62.5 us -> 33.8 us  [swap(): return lax.ppermute(x, axis, [(i, i ^ bit) for i in range(n)])]
    dot_general x4 -> x16, matrix products: 13.4 us -> 28.9 us  [ndot(): lax.dot_general(a, b, (((1,), (1,)), ((), ())), preferred_element_type=F32)]
    ppermute x18, waiting for transfers between devices: 51.5 us -> 62.2 us  [chain(): return lax.ppermute(x, 'fs', pairs)]
    ppermute x18, starting transfers between devices: 43.1 us -> 35.3 us  [chain(): return lax.ppermute(x, 'fs', pairs)]
    concatenate x1 -> x2, other arithmetic: 7.79 us -> 0.14 us  [on_device(): part = jnp.stack([jnp.concatenate(t, 1) for t in zip(*columns_of)])]
    unnamed x52 -> x54, local copies, waits for them, and re-layouts: 9.82 us -> 4.85 us
    another operation x2 -> x4, local copies, waits for them, and re-layouts: 3.75 us -> 7.71 us  [on_device(): part = jnp.stack([jnp.concatenate(t, 1) for t in zip(*columns_of)])]
    dot_general x4, matrix products: 16.4 us -> 12.8 us  [tdot(): lax.dot_general(a, b, (((0,), (0,)), ((), ())), preferred_element_type=F32)]
  transfers between devices with their start and end apart: 29 -> 29, of which waited for: 11 -> 14; matrix products, arithmetic and copies ran while one was open for 28% -> 33% of each run, Pallas kernels for 3% -> 4%
where the time goes in v1:
time: 246 us; the launch traced here: 244 us
  waiting for transfers between devices  96 us (39%)
  starting transfers between devices  49.5 us (20%)
  matrix products  41.8 us (17%)
  other arithmetic  24.3 us (10%)
  local copies, waits for them, and re-layouts  20.6 us (8%)
  Pallas kernels  10.5 us (4%)
    ppermute x18, waiting for transfers between devices, chain(): return lax.ppermute(x, 'fs', pairs)  62.2 us
    ppermute x18, starting transfers between devices, chain(): return lax.ppermute(x, 'fs', pairs)  35.3 us
    ppermute x11, waiting for transfers between devices, swap(): return lax.ppermute(x, axis, [(i, i ^ bit) for i in range(n)])  33.8 us
    dot_general x16, matrix products, ndot(): lax.dot_general(a, b, (((1,), (1,)), ((), ())), preferred_element_type=F32)  28.9 us
    ppermute x11, starting transfers between devices, swap(): return lax.ppermute(x, axis, [(i, i ^ bit) for i in range(n)])  14.2 us
    dot_general x4, matrix products, tdot(): lax.dot_general(a, b, (((0,), (0,)), ((), ())), preferred_element_type=F32)  12.8 us
    pallas_call x1, Pallas kernels, cotangents(): pl.pallas_call(elementwise, grid=(pl.cdiv(columns, LANES),), in_specs=[sm...  10.1 us
    another operation x4, local copies, waits for them, and re-layouts, on_device(): part = jnp.stack([jnp.concatenate(t, 1) for t in zip(*columns_of)])  7.71 us
  transfers between devices with their start and end apart: 29, of which 14 were waited for; matrix products, arithmetic and copies ran while one was open for 33% of the time, Pallas kernels for 4%

profile of v1, /device:TPU:0, one launch (start us, length us, event | category | flops | bytes accessed | tf_op | source)
XLA Modules:
  0.0 244.1 jit_solution(12337818774867964419)
XLA Ops:
  2.2 3.1 %collective-permute-start.11 = (bf16[128,1024]{0,1:T(8,128)(2,1)S(1)}, bf16[128,1024]{0,1:T(8,128)(2,1)S(1)}, u32[]{:S(2)}, u32[]{:S(2)}) collective-permute-start(bf16[128,1024]{0,1:T(8,128)(2,1)S(1)} %bitcast.147), channel_id=1, source_target_pairs={{0,4},{4,0},{8,12},{12,8},{16,20},{20,16},{24,28},{28,24},{1,5},{5... | collective-permute-start | bytes 786440 | tf_op jit(solution)/shard_map/ppermute | solution.py:127
  7.0 5.0 %collective-permute-start = (bf16[2,256,1408]{2,1,0:T(8,128)(2,1)S(1)}, bf16[2,256,1408]{2,1,0:T(8,128)(2,1)}, u32[]{:S(2)}, u32[]{:S(2)}) collective-permute-start(bf16[2,256,1408]{2,1,0:T(8,128)(2,1)S(1)} %shard_map.154), channel_id=1, source_target_pairs={{0,8},{4,12},{8,16},{12,20},{16,24},{20,28},{1,9},{5,13},{9,17},{1... | collective-permute-start | bytes 4325384 | tf_op jit(solution)/shard_map/ppermute | solution.py:132
  13.3 10.1 %shard_map.153 = (bf16[512,1408]{1,0:T(8,128)(2,1)S(1)}, bf16[512,1408]{1,0:T(8,128)(2,1)}, f32[8,1408]{1,0:T(8,128)S(1)}) custom-call(f32[1,1408]{1,0:T(1,128)S(1)} %broadcast_in_dim.26.gs_ref, f32[1,1408]{1,0:T(1,128)S(1)} %broadcast_in_dim.27.vs_ref, f32[3,1408]{1,0:T(4,128)S(1)} %copy-done.5, f32[3,1408]{1,0:T(4,128)S(1)} %copy-done.6, ...), custom_call_target="tpu_custom_call" | custom-call | flops 288358400 | bytes 7208960 | tf_op jit(solution)/shard_map/pallas_call | solution.py:58
  28.4 9.5 %collective-permute-done.12 = bf16[2,1,128,1024]{2,3,0,1:T(8,128)(2,1)} collective-permute-done((bf16[2,1,128,1024]{2,3,0,1:T(8,128)(2,1)}, bf16[2,1,128,1024]{2,3,0,1:T(8,128)(2,1)}, u32[]{:S(2)}, u32[]{:S(2)}) %collective-permute-start.12) | collective-permute-done | bytes 524320 | tf_op jit(solution)/shard_map/ppermute | solution.py:127
  38.0 2.7 %maximum_select_fusion.1 = bf16[2,2,128,1024]{2,3,0,1:T(8,128)(2,1)} fusion(bf16[2,1,128,1024]{2,3,0,1:T(8,128)(2,1)} %get-tuple-element.32, bf16[2,1,128,1024]{2,3,0,1:T(8,128)(2,1)} %collective-permute-done.12, pred[]{:T(512)S(6)} %eq.19), kind=kLoop, calls=%fused_computation.57 | loop fusion | flops 1572864 | bytes 2097153 | tf_op jit(solution)/shard_map/jit(_where)/select_n | solution.py:153
  40.7 2.7 %fusion.13 = bf16[512,256]{0,1:T(8,128)(2,1)} fusion(f32[512,256]{0,1:T(8,128)S(1)} %fusion.25, bf16[512,1408]{1,0:T(8,128)(2,1)} %get-tuple-element.11, bf16[2,256,1408]{2,1,0:T(8,128)(2,1)S(1)} %shard_map.154), kind=kOutput, calls=%fused_computation.43 | convolution fusion | flops 369360896 | bytes 2949120 | tf_op jit(solution)/shard_map/dot_general | solution.py:100
  43.4 14.0 %collective-permute-done.26 = f32[8,1408]{1,0:T(8,128)S(1)} collective-permute-done((f32[8,1408]{1,0:T(8,128)S(1)}, f32[8,1408]{1,0:T(8,128)S(1)}, u32[]{:S(2)}, u32[]{:S(2)}) %collective-permute-start.26) | collective-permute-done | bytes 45088 | tf_op jit(solution)/shard_map/ppermute | solution.py:127
  57.4 2.4 collective-permute-start.27
  61.8 2.6 %collective-permute-start.28 = (f32[8,1408]{1,0:T(8,128)S(1)}, f32[8,1408]{1,0:T(8,128)S(1)}, u32[]{:S(2)}, u32[]{:S(2)}) collective-permute-start(f32[8,1408]{1,0:T(8,128)S(1)} %add.223), channel_id=1, source_target_pairs={{0,16},{4,20},{8,24},{12,28},{16,0},{20,4},{24,8},{28,12},{1,17},{... | collective-permute-start | bytes 135176 | tf_op jit(solution)/shard_map/ppermute | solution.py:127
  73.2 2.8 %fusion.26 = f32[512,256]{0,1:T(8,128)} fusion(bf16[512,1408]{1,0:T(8,128)(2,1)} %collective-permute-done.7, bf16[2,256,1408]{2,1,0:T(8,128)(2,1)S(1)} %shard_map.154), kind=kOutput, calls=%fused_computation.73 | convolution fusion | flops 369098752 | bytes 2686976 | tf_op jit(solution)/shard_map/dot_general | solution.py:100
  79.4 2.3 copy.32
  83.9 3.1 %fusion.40 = f32[1024,1408]{1,0:T(8,128)S(1)} fusion(bf16[512,1024]{1,0:T(8,128)(2,1)} %bitcast.140, bf16[512,1408]{1,0:T(8,128)(2,1)S(1)} %get-tuple-element.10), kind=kOutput, calls=%fused_computation.108 | convolution fusion | flops 1476395008 | bytes 8257536 | tf_op jit(solution)/shard_map/dot_general | solution.py:96
  87.1 3.3 %fusion.41 = f32[1024,1408]{1,0:T(8,128)S(1)} fusion(bf16[512,1024]{1,0:T(8,128)(2,1)S(1)} %bitcast.141, bf16[512,1408]{1,0:T(8,128)(2,1)} %get-tuple-element.11), kind=kOutput, calls=%fused_computation.109 | convolution fusion | flops 1476395008 | bytes 8257536 | tf_op jit(solution)/shard_map/dot_general | solution.py:96
  90.4 6.9 %collective-permute-done.6 = bf16[512,1408]{1,0:T(8,128)(2,1)} collective-permute-done((bf16[512,1408]{1,0:T(8,128)(2,1)S(1)}, bf16[512,1408]{1,0:T(8,128)(2,1)}, u32[]{:S(2)}, u32[]{:S(2)}) %collective-permute-start.6) | collective-permute-done | bytes 1441824 | tf_op jit(solution)/shard_map/ppermute | solution.py:127
  97.3 3.2 %add_convert_fusion.1 = bf16[1024,1408]{1,0:T(8,128)(2,1)S(1)} fusion(f32[1024,1408]{1,0:T(8,128)S(1)} %fusion.40, bf16[512,1024]{1,0:T(8,128)(2,1)S(1)} %bitcast.138, bf16[512,1408]{1,0:T(8,128)(2,1)} %collective-permute-done.6), kind=kOutput, calls=%fused_computation.2 | convolution fusion | flops 1479278592 | bytes 11141120 | tf_op jit(solution)/shard_map/dot_general | solution.py:96
  100.6 3.9 %collective-permute-start.14 = (bf16[256,1408]{1,0:T(8,128)(2,1)S(1)}, bf16[256,1408]{1,0:T(8,128)(2,1)S(1)}, u32[]{:S(2)}, u32[]{:S(2)}) collective-permute-start(bf16[256,1408]{1,0:T(8,128)(2,1)S(1)} %get-tuple-element.28), channel_id=1, source_target_pairs={{0,8},{4,12},{1,9},{5,13},{2,10},{6,14},{3,11},{7,15}} | collective-permute-start | bytes 2162696 | tf_op jit(solution)/shard_map/ppermute | solution.py:132
  104.5 3.2 %add_convert_fusion = bf16[1024,1408]{1,0:T(8,128)(2,1)S(1)} fusion(f32[1024,1408]{1,0:T(8,128)S(1)} %fusion.41, bf16[512,1024]{1,0:T(8,128)(2,1)S(1)} %bitcast.139, bf16[512,1408]{1,0:T(8,128)(2,1)} %collective-permute-done.7), kind=kOutput, calls=%fused_computation.1 | convolution fusion | flops 1479278592 | bytes 11141120 | tf_op jit(solution)/shard_map/dot_general | solution.py:96
  112.0 8.8 %collective-permute-done.14 = bf16[256,1408]{1,0:T(8,128)(2,1)S(1)} collective-permute-done((bf16[256,1408]{1,0:T(8,128)(2,1)S(1)}, bf16[256,1408]{1,0:T(8,128)(2,1)S(1)}, u32[]{:S(2)}, u32[]{:S(2)}) %collective-permute-start.14) | collective-permute-done | bytes 720928 | tf_op jit(solution)/shard_map/ppermute | solution.py:132
  121.7 10.0 %collective-permute-done.20 = bf16[256,1408]{1,0:T(8,128)(2,1)S(1)} collective-permute-done((bf16[256,1408]{1,0:T(8,128)(2,1)S(1)}, bf16[256,1408]{1,0:T(8,128)(2,1)S(1)}, u32[]{:S(2)}, u32[]{:S(2)}) %collective-permute-start.20) | collective-permute-done | bytes 720928 | tf_op jit(solution)/shard_map/ppermute | solution.py:132
  131.7 4.4 %collective-permute-start.15 = (bf16[256,1408]{1,0:T(8,128)(2,1)S(1)}, bf16[256,1408]{1,0:T(8,128)(2,1)S(1)}, u32[]{:S(2)}, u32[]{:S(2)}) collective-permute-start(bf16[256,1408]{1,0:T(8,128)(2,1)S(1)} %fusion.9), channel_id=1, source_target_pairs={{0,8},{4,12},{8,16},{12,20},{1,9},{5,13},{9,17},{13,21},{2,10},{6,... | collective-permute-start | bytes 2162696 | tf_op jit(solution)/shard_map/ppermute | solution.py:132
  148.4 4.2 %collective-permute-done.15 = bf16[256,1408]{1,0:T(8,128)(2,1)S(1)} collective-permute-done((bf16[256,1408]{1,0:T(8,128)(2,1)S(1)}, bf16[256,1408]{1,0:T(8,128)(2,1)S(1)}, u32[]{:S(2)}, u32[]{:S(2)}) %collective-permute-start.15) | collective-permute-done | bytes 720928 | tf_op jit(solution)/shard_map/ppermute | solution.py:132
  155.5 5.7 %collective-permute-done.21 = bf16[256,1408]{1,0:T(8,128)(2,1)S(1)} collective-permute-done((bf16[256,1408]{1,0:T(8,128)(2,1)S(1)}, bf16[256,1408]{1,0:T(8,128)(2,1)S(1)}, u32[]{:S(2)}, u32[]{:S(2)}) %collective-permute-start.21) | collective-permute-done | bytes 720928 | tf_op jit(solution)/shard_map/ppermute | solution.py:132
  165.8 2.5 %fusion.32 = f32[512,256]{0,1:T(8,128)S(1)} fusion(bf16[512,1408]{1,0:T(8,128)(2,1)} %get-tuple-element.11, bf16[2,256,1408]{2,1,0:T(8,128)(2,1)S(1)} %broadcast_select_fusion), kind=kOutput, calls=%fused_computation.79 | convolution fusion | flops 369098752 | bytes 2686976 | tf_op jit(solution)/shard_map/dot_general | solution.py:100
  168.9 6.4 %collective-permute-done.3 = bf16[2,256,1408]{2,1,0:T(8,128)(2,1)S(1)} collective-permute-done((bf16[2,256,1408]{2,1,0:T(8,128)(2,1)}, bf16[2,256,1408]{2,1,0:T(8,128)(2,1)S(1)}, u32[]{:S(2)}, u32[]{:S(2)}) %collective-permute-start.3) | collective-permute-done | bytes 1441824 | tf_op jit(solution)/shard_map/ppermute | solution.py:132
  175.5 2.5 %fusion.28 = f32[512,256]{0,1:T(8,128)S(1)} fusion(bf16[512,1408]{1,0:T(8,128)(2,1)} %get-tuple-element.11, bf16[2,256,1408]{2,1,0:T(8,128)(2,1)S(1)} %broadcast_select_fusion.2), kind=kOutput, calls=%fused_computation.75 | convolution fusion | flops 369098752 | bytes 2686976 | tf_op jit(solution)/shard_map/dot_general | solution.py:100
  179.3 2.5 %copy.22 = bf16[1,2,2,128,1024]{4,3,1,0,2:T(8,128)(2,1)} copy(bf16[1,2,2,128,1024]{3,2,1,4,0:T(2,128)(2,1)S(1)} %stack.53) | data formatting | bytes 2097152 | tf_op jit(solution)/shard_map/stack | solution.py:208
  191.3 3.8 %copy.23 = bf16[1,2,2,128,1024]{4,3,1,0,2:T(8,128)(2,1)} copy(bf16[1,2,2,128,1024]{3,2,1,4,0:T(2,128)(2,1)} %stack.54) | data formatting | bytes 2097152 | tf_op jit(solution)/shard_map/stack | solution.py:208
  197.9 3.0 %collective-permute-start.16 = (bf16[256,1408]{1,0:T(8,128)(2,1)}, bf16[256,1408]{1,0:T(8,128)(2,1)S(1)}, u32[]{:S(2)}, u32[]{:S(2)}) collective-permute-start(bf16[256,1408]{1,0:T(8,128)(2,1)} %get-tuple-element.26), channel_id=1, source_target_pairs={{0,8},{4,12},{8,16},{12,20},{16,24},{20,28},{1,9},{5,13},{9,17},{1... | collective-permute-start | bytes 2162696 | tf_op jit(solution)/shard_map/ppermute | solution.py:132
  210.5 7.2 %collective-permute-done.16 = bf16[256,1408]{1,0:T(8,128)(2,1)S(1)} collective-permute-done((bf16[256,1408]{1,0:T(8,128)(2,1)}, bf16[256,1408]{1,0:T(8,128)(2,1)S(1)}, u32[]{:S(2)}, u32[]{:S(2)}) %collective-permute-start.16) | collective-permute-done | bytes 720928 | tf_op jit(solution)/shard_map/ppermute | solution.py:132
  217.6 7.5 %collective-permute-done.19 = bf16[256,1408]{1,0:T(8,128)(2,1)S(1)} collective-permute-done((bf16[256,1408]{1,0:T(8,128)(2,1)S(1)}, bf16[256,1408]{1,0:T(8,128)(2,1)S(1)}, u32[]{:S(2)}, u32[]{:S(2)}) %collective-permute-start.19) | collective-permute-done | bytes 720928 | tf_op jit(solution)/shard_map/ppermute | solution.py:132
  227.4 5.2 %collective-permute-done.22 = bf16[256,1408]{1,0:T(8,128)(2,1)S(1)} collective-permute-done((bf16[256,1408]{1,0:T(8,128)(2,1)}, bf16[256,1408]{1,0:T(8,128)(2,1)S(1)}, u32[]{:S(2)}, u32[]{:S(2)}) %collective-permute-start.22) | collective-permute-done | bytes 720928 | tf_op jit(solution)/shard_map/ppermute | solution.py:132
  232.6 7.2 %collective-permute-done.25 = bf16[256,1408]{1,0:T(8,128)(2,1)S(1)} collective-permute-done((bf16[256,1408]{1,0:T(8,128)(2,1)S(1)}, bf16[256,1408]{1,0:T(8,128)(2,1)S(1)}, u32[]{:S(2)}, u32[]{:S(2)}) %collective-permute-start.25) | collective-permute-done | bytes 720928 | tf_op jit(solution)/shard_map/ppermute | solution.py:132
  (151 shorter events, 81.1 us)
Async XLA Ops:
  2.2 21.8 %collective-permute-start.11 = (bf16[128,1024]{0,1:T(8,128)(2,1)S(1)}, bf16[128,1024]{0,1:T(8,128)(2,1)S(1)}, u32[]{:S(2)}, u32[]{:S(2)}) collective-permute-start(bf16[128,1024]{0,1:T(8,128)(2,1)S(1)} %bitcast.147), channel_id=1, source_target_pairs={{0,4},{4,0},{8,12},{12,8},{16,20},{20,16},{24,28},{28,24},{1,5},{5... | collective-permute-start | bytes 786440 | tf_op jit(solution)/shard_map/ppermute | solution.py:127
  7.0 63.2 %collective-permute-start = (bf16[2,256,1408]{2,1,0:T(8,128)(2,1)S(1)}, bf16[2,256,1408]{2,1,0:T(8,128)(2,1)}, u32[]{:S(2)}, u32[]{:S(2)}) collective-permute-start(bf16[2,256,1408]{2,1,0:T(8,128)(2,1)S(1)} %shard_map.154), channel_id=1, source_target_pairs={{0,8},{4,12},{8,16},{12,20},{16,24},{20,28},{1,9},{5,13},{9,17},{1... | collective-permute-start | bytes 4325384 | tf_op jit(solution)/shard_map/ppermute | solution.py:132
  12.0 60.0 %collective-permute-start.1 = (bf16[2,256,1408]{2,1,0:T(8,128)(2,1)S(1)}, bf16[2,256,1408]{2,1,0:T(8,128)(2,1)}, u32[]{:S(2)}, u32[]{:S(2)}) collective-permute-start(bf16[2,256,1408]{2,1,0:T(8,128)(2,1)S(1)} %shard_map.154), channel_id=1, source_target_pairs={{8,0},{12,4},{16,8},{20,12},{24,16},{28,20},{9,1},{13,5},{17,9},{2... | collective-permute-start | bytes 4325384 | tf_op jit(solution)/shard_map/ppermute | solution.py:132
  23.4 49.8 %collective-permute-start.7 = (bf16[512,1408]{1,0:T(8,128)(2,1)}, bf16[512,1408]{1,0:T(8,128)(2,1)}, u32[]{:S(2)}, u32[]{:S(2)}) collective-permute-start(bf16[512,1408]{1,0:T(8,128)(2,1)} %get-tuple-element.11), channel_id=1, source_target_pairs={{0,4},{4,0},{8,12},{12,8},{16,20},{20,16},{24,28},{28,24},{1,5},{5... | collective-permute-start | bytes 4325384 | tf_op jit(solution)/shard_map/ppermute | solution.py:127
  24.8 13.1 %collective-permute-start.12 = (bf16[2,1,128,1024]{2,3,0,1:T(8,128)(2,1)}, bf16[2,1,128,1024]{2,3,0,1:T(8,128)(2,1)}, u32[]{:S(2)}, u32[]{:S(2)}) collective-permute-start(bf16[2,1,128,1024]{2,3,0,1:T(8,128)(2,1)} %get-tuple-element.32), channel_id=1, source_target_pairs={{0,2},{1,3},{2,0},{3,1},{4,6},{5,7},{6,4},{7,5},{8,10},{9,11},{10,... | collective-permute-start | bytes 1572872 | tf_op jit(solution)/shard_map/ppermute | solution.py:127
  26.3 31.1 %collective-permute-start.26 = (f32[8,1408]{1,0:T(8,128)S(1)}, f32[8,1408]{1,0:T(8,128)S(1)}, u32[]{:S(2)}, u32[]{:S(2)}) collective-permute-start(f32[8,1408]{1,0:T(8,128)S(1)} %get-tuple-element.12), channel_id=1, source_target_pairs={{0,4},{4,0},{8,12},{12,8},{16,20},{20,16},{24,28},{28,24},{1,5},{5... | collective-permute-start | bytes 135176 | tf_op jit(solution)/shard_map/ppermute | solution.py:127
  40.7 35.3 %collective-permute-start.13 = (bf16[2,2,128,1024]{2,3,0,1:T(8,128)(2,1)}, bf16[2,2,128,1024]{2,3,0,1:T(8,128)(2,1)}, u32[]{:S(2)}, u32[]{:S(2)}) collective-permute-start(bf16[2,2,128,1024]{2,3,0,1:T(8,128)(2,1)} %maximum_select_fusion.1), channel_id=1, source_target_pairs={{0,1},{1,0},{2,3},{3,2},{4,5},{5,4},{6,7},{7,6},{8,9},{9,8},{10,11... | collective-permute-start | bytes 3145736 | tf_op jit(solution)/shard_map/ppermute | solution.py:127
  57.4 4.5 %collective-permute-start.27 = (f32[8,1408]{1,0:T(8,128)S(1)}, f32[8,1408]{1,0:T(8,128)S(1)}, u32[]{:S(2)}, u32[]{:S(2)}) collective-permute-start(f32[8,1408]{1,0:T(8,128)S(1)} %add.222), channel_id=1, source_target_pairs={{0,8},{4,12},{8,0},{12,4},{16,24},{20,28},{24,16},{28,20},{1,9},{5... | collective-permute-start | bytes 135176 | tf_op jit(solution)/shard_map/ppermute | solution.py:127
  61.8 5.0 %collective-permute-start.28 = (f32[8,1408]{1,0:T(8,128)S(1)}, f32[8,1408]{1,0:T(8,128)S(1)}, u32[]{:S(2)}, u32[]{:S(2)}) collective-permute-start(f32[8,1408]{1,0:T(8,128)S(1)} %add.223), channel_id=1, source_target_pairs={{0,16},{4,20},{8,24},{12,28},{16,0},{20,4},{24,8},{28,12},{1,17},{... | collective-permute-start | bytes 135176 | tf_op jit(solution)/shard_map/ppermute | solution.py:127
  67.5 29.8 %collective-permute-start.6 = (bf16[512,1408]{1,0:T(8,128)(2,1)S(1)}, bf16[512,1408]{1,0:T(8,128)(2,1)}, u32[]{:S(2)}, u32[]{:S(2)}) collective-permute-start(bf16[512,1408]{1,0:T(8,128)(2,1)S(1)} %get-tuple-element.10), channel_id=1, source_target_pairs={{0,4},{4,0},{8,12},{12,8},{16,20},{20,16},{24,28},{28,24},{1,5},{5... | collective-permute-start | bytes 4325384 | tf_op jit(solution)/shard_map/ppermute | solution.py:127
  70.2 66.1 %collective-permute-start.4 = (bf16[2,256,1408]{2,1,0:T(8,128)(2,1)}, bf16[2,256,1408]{2,1,0:T(8,128)(2,1)}, u32[]{:S(2)}, u32[]{:S(2)}) collective-permute-start(bf16[2,256,1408]{2,1,0:T(8,128)(2,1)} %collective-permute-done), channel_id=1, source_target_pairs={{8,16},{12,20},{16,24},{20,28},{9,17},{13,21},{17,25},{21,29},{10,... | collective-permute-start | bytes 4325384 | tf_op jit(solution)/shard_map/ppermute | solution.py:132
  71.9 66.3 %collective-permute-start.2 = (bf16[2,256,1408]{2,1,0:T(8,128)(2,1)}, bf16[2,256,1408]{2,1,0:T(8,128)(2,1)}, u32[]{:S(2)}, u32[]{:S(2)}) collective-permute-start(bf16[2,256,1408]{2,1,0:T(8,128)(2,1)} %collective-permute-done.1), channel_id=1, source_target_pairs={{8,0},{12,4},{16,8},{20,12},{9,1},{13,5},{17,9},{21,13},{10,2},{14... | collective-permute-start | bytes 4325384 | tf_op jit(solution)/shard_map/ppermute | solution.py:132
  100.5 52.1 %copy-start.9 = (bf16[1024,1408]{1,0:T(8,128)(2,1)}, bf16[1024,1408]{1,0:T(8,128)(2,1)S(1)}, u32[]{:S(2)}) copy-start(bf16[1024,1408]{1,0:T(8,128)(2,1)S(1)} %add_convert_fusion.1) | copy-start | bytes 8650756
  100.6 20.2 %collective-permute-start.14 = (bf16[256,1408]{1,0:T(8,128)(2,1)S(1)}, bf16[256,1408]{1,0:T(8,128)(2,1)S(1)}, u32[]{:S(2)}, u32[]{:S(2)}) collective-permute-start(bf16[256,1408]{1,0:T(8,128)(2,1)S(1)} %get-tuple-element.28), channel_id=1, source_target_pairs={{0,8},{4,12},{1,9},{5,13},{2,10},{6,14},{3,11},{7,15}} | collective-permute-start | bytes 2162696 | tf_op jit(solution)/shard_map/ppermute | solution.py:132
  107.7 53.5 %copy-start.7 = (bf16[1024,1408]{1,0:T(8,128)(2,1)}, bf16[1024,1408]{1,0:T(8,128)(2,1)S(1)}, u32[]{:S(2)}) copy-start(bf16[1024,1408]{1,0:T(8,128)(2,1)S(1)} %add_convert_fusion) | copy-start | bytes 8650756
  107.9 23.8 %collective-permute-start.20 = (bf16[256,1408]{1,0:T(8,128)(2,1)S(1)}, bf16[256,1408]{1,0:T(8,128)(2,1)S(1)}, u32[]{:S(2)}, u32[]{:S(2)}) collective-permute-start(bf16[256,1408]{1,0:T(8,128)(2,1)S(1)} %get-tuple-element.24), channel_id=1, source_target_pairs={{0,8},{4,12},{1,9},{5,13},{2,10},{6,14},{3,11},{7,15}} | collective-permute-start | bytes 2162696 | tf_op jit(solution)/shard_map/ppermute | solution.py:132
  111.3 35.7 %collective-permute-start.17 = (bf16[256,1408]{1,0:T(8,128)(2,1)S(1)}, bf16[256,1408]{1,0:T(8,128)(2,1)S(1)}, u32[]{:S(2)}, u32[]{:S(2)}) collective-permute-start(bf16[256,1408]{1,0:T(8,128)(2,1)S(1)} %get-tuple-element.29), channel_id=1, source_target_pairs={{24,16},{28,20},{25,17},{29,21},{26,18},{30,22},{27,19},{31,23}} | collective-permute-start | bytes 2162696 | tf_op jit(solution)/shard_map/ppermute | solution.py:132
  120.8 34.8 %collective-permute-start.23 = (bf16[256,1408]{1,0:T(8,128)(2,1)S(1)}, bf16[256,1408]{1,0:T(8,128)(2,1)S(1)}, u32[]{:S(2)}, u32[]{:S(2)}) collective-permute-start(bf16[256,1408]{1,0:T(8,128)(2,1)S(1)} %get-tuple-element.25), channel_id=1, source_target_pairs={{24,16},{28,20},{25,17},{29,21},{26,18},{30,22},{27,19},{31,23}} | collective-permute-start | bytes 2162696 | tf_op jit(solution)/shard_map/ppermute | solution.py:132
  131.7 20.9 %collective-permute-start.15 = (bf16[256,1408]{1,0:T(8,128)(2,1)S(1)}, bf16[256,1408]{1,0:T(8,128)(2,1)S(1)}, u32[]{:S(2)}, u32[]{:S(2)}) collective-permute-start(bf16[256,1408]{1,0:T(8,128)(2,1)S(1)} %fusion.9), channel_id=1, source_target_pairs={{0,8},{4,12},{8,16},{12,20},{1,9},{5,13},{9,17},{13,21},{2,10},{6,... | collective-permute-start | bytes 2162696 | tf_op jit(solution)/shard_map/ppermute | solution.py:132
  136.3 25.0 %collective-permute-start.21 = (bf16[256,1408]{1,0:T(8,128)(2,1)S(1)}, bf16[256,1408]{1,0:T(8,128)(2,1)S(1)}, u32[]{:S(2)}, u32[]{:S(2)}) collective-permute-start(bf16[256,1408]{1,0:T(8,128)(2,1)S(1)} %fusion.3), channel_id=1, source_target_pairs={{0,8},{4,12},{8,16},{12,20},{1,9},{5,13},{9,17},{13,21},{2,10},{6,... | collective-permute-start | bytes 2162696 | tf_op jit(solution)/shard_map/ppermute | solution.py:132
  142.3 22.0 %collective-permute-start.5 = (bf16[2,256,1408]{2,1,0:T(8,128)(2,1)}, bf16[2,256,1408]{2,1,0:T(8,128)(2,1)S(1)}, u32[]{:S(2)}, u32[]{:S(2)}) collective-permute-start(bf16[2,256,1408]{2,1,0:T(8,128)(2,1)} %collective-permute-done.4), channel_id=1, source_target_pairs={{16,24},{20,28},{17,25},{21,29},{18,26},{22,30},{19,27},{23,31}} | collective-permute-start | bytes 4325384 | tf_op jit(solution)/shard_map/ppermute | solution.py:132
  147.1 28.2 %collective-permute-start.3 = (bf16[2,256,1408]{2,1,0:T(8,128)(2,1)}, bf16[2,256,1408]{2,1,0:T(8,128)(2,1)S(1)}, u32[]{:S(2)}, u32[]{:S(2)}) collective-permute-start(bf16[2,256,1408]{2,1,0:T(8,128)(2,1)} %collective-permute-done.2), channel_id=1, source_target_pairs={{8,0},{12,4},{9,1},{13,5},{10,2},{14,6},{11,3},{15,7}} | collective-permute-start | bytes 4325384 | tf_op jit(solution)/shard_map/ppermute | solution.py:132
  154.0 48.8 %collective-permute-start.18 = (bf16[256,1408]{1,0:T(8,128)(2,1)}, bf16[256,1408]{1,0:T(8,128)(2,1)}, u32[]{:S(2)}, u32[]{:S(2)}) collective-permute-start(bf16[256,1408]{1,0:T(8,128)(2,1)} %get-tuple-element.27), channel_id=1, source_target_pairs={{16,8},{20,12},{24,16},{28,20},{17,9},{21,13},{25,17},{29,21},{18,... | collective-permute-start | bytes 2162696 | tf_op jit(solution)/shard_map/ppermute | solution.py:132
  162.8 42.8 %collective-permute-start.24 = (bf16[256,1408]{1,0:T(8,128)(2,1)}, bf16[256,1408]{1,0:T(8,128)(2,1)}, u32[]{:S(2)}, u32[]{:S(2)}) collective-permute-start(bf16[256,1408]{1,0:T(8,128)(2,1)} %get-tuple-element.23), channel_id=1, source_target_pairs={{16,8},{20,12},{24,16},{28,20},{17,9},{21,13},{25,17},{29,21},{18,... | collective-permute-start | bytes 2162696 | tf_op jit(solution)/shard_map/ppermute | solution.py:132
  191.3 11.5 %copy-start.10 = (bf16[1024,1408]{1,0:T(8,128)(2,1)S(1)}, bf16[1024,1408]{1,0:T(8,128)(2,1)}, u32[]{:S(2)}) copy-start(bf16[1024,1408]{1,0:T(8,128)(2,1)} %copy-done.9) | copy-start | bytes 8650756
  196.6 11.8 %collective-permute-start.8 = (bf16[2,2,128,1024]{3,2,1,0:T(8,128)(2,1)S(1)}, bf16[2,2,128,1024]{3,2,1,0:T(8,128)(2,1)S(1)}, u32[]{:S(2)}, u32[]{:S(2)}) collective-permute-start(bf16[2,2,128,1024]{3,2,1,0:T(8,128)(2,1)S(1)} %fusion.22), channel_id=1, source_target_pairs={{0,1},{1,0},{2,3},{3,2},{4,5},{5,4},{6,7},{7,6},{8,9},{9,8},{10,11... | collective-permute-start | bytes 3145736 | tf_op jit(solution)/shard_map/ppermute | solution.py:127
  197.9 19.7 %collective-permute-start.16 = (bf16[256,1408]{1,0:T(8,128)(2,1)}, bf16[256,1408]{1,0:T(8,128)(2,1)S(1)}, u32[]{:S(2)}, u32[]{:S(2)}) collective-permute-start(bf16[256,1408]{1,0:T(8,128)(2,1)} %get-tuple-element.26), channel_id=1, source_target_pairs={{0,8},{4,12},{8,16},{12,20},{16,24},{20,28},{1,9},{5,13},{9,17},{1... | collective-permute-start | bytes 2162696 | tf_op jit(solution)/shard_map/ppermute | solution.py:132
  200.9 31.7 %collective-permute-start.22 = (bf16[256,1408]{1,0:T(8,128)(2,1)}, bf16[256,1408]{1,0:T(8,128)(2,1)S(1)}, u32[]{:S(2)}, u32[]{:S(2)}) collective-permute-start(bf16[256,1408]{1,0:T(8,128)(2,1)} %get-tuple-element.22), channel_id=1, source_target_pairs={{0,8},{4,12},{8,16},{12,20},{16,24},{20,28},{1,9},{5,13},{9,17},{1... | collective-permute-start | bytes 2162696 | tf_op jit(solution)/shard_map/ppermute | solution.py:132
  204.1 21.0 %collective-permute-start.19 = (bf16[256,1408]{1,0:T(8,128)(2,1)S(1)}, bf16[256,1408]{1,0:T(8,128)(2,1)S(1)}, u32[]{:S(2)}, u32[]{:S(2)}) collective-permute-start(bf16[256,1408]{1,0:T(8,128)(2,1)S(1)} %fusion.8), channel_id=1, source_target_pairs={{8,0},{12,4},{16,8},{20,12},{24,16},{28,20},{9,1},{13,5},{17,9},{2... | collective-permute-start | bytes 2162696 | tf_op jit(solution)/shard_map/ppermute | solution.py:132
  206.9 33.0 %collective-permute-start.25 = (bf16[256,1408]{1,0:T(8,128)(2,1)S(1)}, bf16[256,1408]{1,0:T(8,128)(2,1)S(1)}, u32[]{:S(2)}, u32[]{:S(2)}) collective-permute-start(bf16[256,1408]{1,0:T(8,128)(2,1)S(1)} %fusion.2), channel_id=1, source_target_pairs={{8,0},{12,4},{16,8},{20,12},{24,16},{28,20},{9,1},{13,5},{17,9},{2... | collective-permute-start | bytes 2162696 | tf_op jit(solution)/shard_map/ppermute | solution.py:132
  208.9 17.6 %collective-permute-start.9 = (bf16[2,1,128,1024]{3,2,1,0:T(8,128)(2,1)S(1)}, bf16[2,1,128,1024]{3,2,1,0:T(8,128)(2,1)S(1)}, u32[]{:S(2)}, u32[]{:S(2)}) collective-permute-start(bf16[2,1,128,1024]{3,2,1,0:T(8,128)(2,1)S(1)} %constant_dynamic-slice_fusion.2), channel_id=1, source_target_pairs={{0,2},{1,3},{2,0},{3,1},{4,6},{5,7},{6,4},{7,5},{8,10},{9,11},{10,... | collective-permute-start | bytes 1572872 | tf_op jit(solution)/shard_map/ppermute | solution.py:127
  226.8 14.8 %collective-permute-start.10 = (bf16[128,1024]{1,0:T(8,128)(2,1)S(1)}, bf16[128,1024]{1,0:T(8,128)(2,1)S(1)}, u32[]{:S(2)}, u32[]{:S(2)}) collective-permute-start(bf16[128,1024]{1,0:T(8,128)(2,1)S(1)} %get-tuple-element.37), channel_id=1, source_target_pairs={{0,4},{4,0},{8,12},{12,8},{16,20},{20,16},{24,28},{28,24},{1,5},{5... | collective-permute-start | bytes 786440 | tf_op jit(solution)/shard_map/ppermute | solution.py:127
  (23 other events, 108.7 us)

commit v2 on v1

--- a/solution.py
+++ b/solution.py
@@ -158,10 +158,10 @@
         gate_cot, value_cot, sums = cotangents(
             gate_scale, value_scale, conv_gate, conv_value, gate_pre, value_pre, grad_out
         )
-        bit = 1
-        while bit < n_fs:
+        bit = n_fs // 2
+        while bit:
             sums = sums + swap(sums, "fs", bit, n_fs)
-            bit *= 2
+            bit //= 2
 
         gate_theirs = swap(gate_cot, "fs", 1, n_fs)
         value_theirs = swap(value_cot, "fs", 1, n_fs)

time: 246 us -> 243 us (0.988)
    ppermute x11, waiting for transfers between devices: 33.8 us -> 29 us  [swap(): return lax.ppermute(x, axis, [(i, i ^ bit) for i in range(n)])]
    ppermute x18, waiting for transfers between devices: 62.2 us -> 66.8 us  [chain(): return lax.ppermute(x, 'fs', pairs)]
where the time goes in v2:
time: 243 us; the launch traced here: 242 us
  waiting for transfers between devices  95.7 us (39%)
  starting transfers between devices  47.6 us (20%)
  matrix products  41.8 us (17%)
  other arithmetic  24.3 us (10%)
  local copies, waits for them, and re-layouts  20.5 us (8%)
  Pallas kernels  10.5 us (4%)
    ppermute x18, waiting for transfers between devices, chain(): return lax.ppermute(x, 'fs', pairs)  66.8 us
    ppermute x18, starting transfers between devices, chain(): return lax.ppermute(x, 'fs', pairs)  35.6 us
    ppermute x11, waiting for transfers between devices, swap(): return lax.ppermute(x, axis, [(i, i ^ bit) for i in range(n)])  29 us
    dot_general x16, matrix products, ndot(): lax.dot_general(a, b, (((1,), (1,)), ((), ())), preferred_element_type=F32)  28.9 us
    dot_general x4, matrix products, tdot(): lax.dot_general(a, b, (((0,), (0,)), ((), ())), preferred_element_type=F32)  12.8 us
    ppermute x11, starting transfers between devices, swap(): return lax.ppermute(x, axis, [(i, i ^ bit) for i in range(n)])  12 us
    pallas_call x1, Pallas kernels, cotangents(): pl.pallas_call(elementwise, grid=(pl.cdiv(columns, LANES),), in_specs=[sm...  10.1 us
    another operation x4, local copies, waits for them, and re-layouts, on_device(): part = jnp.stack([jnp.concatenate(t, 1) for t in zip(*columns_of)])  7.71 us
  transfers between devices with their start and end apart: 29, of which 14 were waited for; matrix products, arithmetic and copies ran while one was open for 33% of the time, Pallas kernels for 4%

profile of v2, /device:TPU:0, one launch (start us, length us, event | category | flops | bytes accessed | tf_op | source)
XLA Modules:
  0.0 241.9 jit_solution(5125218170514425771)
XLA Ops:
  2.2 3.1 %collective-permute-start.11 = (bf16[128,1024]{0,1:T(8,128)(2,1)S(1)}, bf16[128,1024]{0,1:T(8,128)(2,1)S(1)}, u32[]{:S(2)}, u32[]{:S(2)}) collective-permute-start(bf16[128,1024]{0,1:T(8,128)(2,1)S(1)} %bitcast.147), channel_id=1, source_target_pairs={{0,4},{4,0},{8,12},{12,8},{16,20},{20,16},{24,28},{28,24},{1,5},{5... | collective-permute-start | bytes 786440 | tf_op jit(solution)/shard_map/ppermute | solution.py:127
  7.0 5.0 %collective-permute-start = (bf16[2,256,1408]{2,1,0:T(8,128)(2,1)S(1)}, bf16[2,256,1408]{2,1,0:T(8,128)(2,1)}, u32[]{:S(2)}, u32[]{:S(2)}) collective-permute-start(bf16[2,256,1408]{2,1,0:T(8,128)(2,1)S(1)} %shard_map.154), channel_id=1, source_target_pairs={{0,8},{4,12},{8,16},{12,20},{16,24},{20,28},{1,9},{5,13},{9,17},{1... | collective-permute-start | bytes 4325384 | tf_op jit(solution)/shard_map/ppermute | solution.py:132
  13.3 10.1 %shard_map.153 = (bf16[512,1408]{1,0:T(8,128)(2,1)S(1)}, bf16[512,1408]{1,0:T(8,128)(2,1)}, f32[8,1408]{1,0:T(8,128)S(1)}) custom-call(f32[1,1408]{1,0:T(1,128)S(1)} %broadcast_in_dim.26.gs_ref, f32[1,1408]{1,0:T(1,128)S(1)} %broadcast_in_dim.27.vs_ref, f32[3,1408]{1,0:T(4,128)S(1)} %copy-done.5, f32[3,1408]{1,0:T(4,128)S(1)} %copy-done.6, ...), custom_call_target="tpu_custom_call" | custom-call | flops 288358400 | bytes 7208960 | tf_op jit(solution)/shard_map/pallas_call | solution.py:58
  26.3 2.5 %collective-permute-start.26 = (f32[8,1408]{1,0:T(8,128)S(1)}, f32[8,1408]{1,0:T(8,128)S(1)}, u32[]{:S(2)}, u32[]{:S(2)}) collective-permute-start(f32[8,1408]{1,0:T(8,128)S(1)} %get-tuple-element.12), channel_id=1, source_target_pairs={{0,16},{4,20},{8,24},{12,28},{16,0},{20,4},{24,8},{28,12},{1,17},{... | collective-permute-start | bytes 135176 | tf_op jit(solution)/shard_map/ppermute | solution.py:127
  29.4 8.6 %collective-permute-done.12 = bf16[2,1,128,1024]{2,3,0,1:T(8,128)(2,1)} collective-permute-done((bf16[2,1,128,1024]{2,3,0,1:T(8,128)(2,1)}, bf16[2,1,128,1024]{2,3,0,1:T(8,128)(2,1)}, u32[]{:S(2)}, u32[]{:S(2)}) %collective-permute-start.12) | collective-permute-done | bytes 524320 | tf_op jit(solution)/shard_map/ppermute | solution.py:127
  38.0 2.7 %maximum_select_fusion.1 = bf16[2,2,128,1024]{2,3,0,1:T(8,128)(2,1)} fusion(bf16[2,1,128,1024]{2,3,0,1:T(8,128)(2,1)} %get-tuple-element.32, bf16[2,1,128,1024]{2,3,0,1:T(8,128)(2,1)} %collective-permute-done.12, pred[]{:T(512)S(6)} %eq.19), kind=kLoop, calls=%fused_computation.57 | loop fusion | flops 1572864 | bytes 2097153 | tf_op jit(solution)/shard_map/jit(_where)/select_n | solution.py:153
  40.7 2.7 %fusion.13 = bf16[512,256]{0,1:T(8,128)(2,1)} fusion(f32[512,256]{0,1:T(8,128)S(1)} %fusion.25, bf16[512,1408]{1,0:T(8,128)(2,1)} %get-tuple-element.11, bf16[2,256,1408]{2,1,0:T(8,128)(2,1)S(1)} %shard_map.154), kind=kOutput, calls=%fused_computation.43 | convolution fusion | flops 369360896 | bytes 2949120 | tf_op jit(solution)/shard_map/dot_general | solution.py:100
  43.4 4.5 %collective-permute-done.26 = f32[8,1408]{1,0:T(8,128)S(1)} collective-permute-done((f32[8,1408]{1,0:T(8,128)S(1)}, f32[8,1408]{1,0:T(8,128)S(1)}, u32[]{:S(2)}, u32[]{:S(2)}) %collective-permute-start.26) | collective-permute-done | bytes 45088 | tf_op jit(solution)/shard_map/ppermute | solution.py:127
  49.6 2.4 collective-permute-done.27
  53.1 4.3 %collective-permute-done.28 = f32[8,1408]{1,0:T(8,128)S(1)} collective-permute-done((f32[8,1408]{1,0:T(8,128)S(1)}, f32[8,1408]{1,0:T(8,128)S(1)}, u32[]{:S(2)}, u32[]{:S(2)}) %collective-permute-start.28) | collective-permute-done | bytes 45088 | tf_op jit(solution)/shard_map/ppermute | solution.py:127
  63.8 2.8 %fusion.26 = f32[512,256]{0,1:T(8,128)} fusion(bf16[512,1408]{1,0:T(8,128)(2,1)} %collective-permute-done.7, bf16[2,256,1408]{2,1,0:T(8,128)(2,1)S(1)} %shard_map.154), kind=kOutput, calls=%fused_computation.73 | convolution fusion | flops 369098752 | bytes 2686976 | tf_op jit(solution)/shard_map/dot_general | solution.py:100
  74.5 3.1 %fusion.40 = f32[1024,1408]{1,0:T(8,128)S(1)} fusion(bf16[512,1024]{1,0:T(8,128)(2,1)} %bitcast.140, bf16[512,1408]{1,0:T(8,128)(2,1)S(1)} %get-tuple-element.10), kind=kOutput, calls=%fused_computation.108 | convolution fusion | flops 1476395008 | bytes 8257536 | tf_op jit(solution)/shard_map/dot_general | solution.py:96
  77.6 3.3 %fusion.41 = f32[1024,1408]{1,0:T(8,128)S(1)} fusion(bf16[512,1024]{1,0:T(8,128)(2,1)S(1)} %bitcast.141, bf16[512,1408]{1,0:T(8,128)(2,1)} %get-tuple-element.11), kind=kOutput, calls=%fused_computation.109 | convolution fusion | flops 1476395008 | bytes 8257536 | tf_op jit(solution)/shard_map/dot_general | solution.py:96
  80.9 9.2 %collective-permute-done.6 = bf16[512,1408]{1,0:T(8,128)(2,1)} collective-permute-done((bf16[512,1408]{1,0:T(8,128)(2,1)S(1)}, bf16[512,1408]{1,0:T(8,128)(2,1)}, u32[]{:S(2)}, u32[]{:S(2)}) %collective-permute-start.6) | collective-permute-done | bytes 1441824 | tf_op jit(solution)/shard_map/ppermute | solution.py:127
  90.1 3.2 %add_convert_fusion.1 = bf16[1024,1408]{1,0:T(8,128)(2,1)S(1)} fusion(f32[1024,1408]{1,0:T(8,128)S(1)} %fusion.40, bf16[512,1024]{1,0:T(8,128)(2,1)S(1)} %bitcast.138, bf16[512,1408]{1,0:T(8,128)(2,1)} %collective-permute-done.6), kind=kOutput, calls=%fused_computation.2 | convolution fusion | flops 1479278592 | bytes 11141120 | tf_op jit(solution)/shard_map/dot_general | solution.py:96
  93.5 4.2 %collective-permute-start.14 = (bf16[256,1408]{1,0:T(8,128)(2,1)S(1)}, bf16[256,1408]{1,0:T(8,128)(2,1)S(1)}, u32[]{:S(2)}, u32[]{:S(2)}) collective-permute-start(bf16[256,1408]{1,0:T(8,128)(2,1)S(1)} %get-tuple-element.28), channel_id=1, source_target_pairs={{0,8},{4,12},{1,9},{5,13},{2,10},{6,14},{3,11},{7,15}} | collective-permute-start | bytes 2162696 | tf_op jit(solution)/shard_map/ppermute | solution.py:132
  97.7 3.2 %add_convert_fusion = bf16[1024,1408]{1,0:T(8,128)(2,1)S(1)} fusion(f32[1024,1408]{1,0:T(8,128)S(1)} %fusion.41, bf16[512,1024]{1,0:T(8,128)(2,1)S(1)} %bitcast.139, bf16[512,1408]{1,0:T(8,128)(2,1)} %collective-permute-done.7), kind=kOutput, calls=%fused_computation.1 | convolution fusion | flops 1479278592 | bytes 11141120 | tf_op jit(solution)/shard_map/dot_general | solution.py:96
  105.2 8.8 %collective-permute-done.14 = bf16[256,1408]{1,0:T(8,128)(2,1)S(1)} collective-permute-done((bf16[256,1408]{1,0:T(8,128)(2,1)S(1)}, bf16[256,1408]{1,0:T(8,128)(2,1)S(1)}, u32[]{:S(2)}, u32[]{:S(2)}) %collective-permute-start.14) | collective-permute-done | bytes 720928 | tf_op jit(solution)/shard_map/ppermute | solution.py:132
  114.9 11.0 %collective-permute-done.20 = bf16[256,1408]{1,0:T(8,128)(2,1)S(1)} collective-permute-done((bf16[256,1408]{1,0:T(8,128)(2,1)S(1)}, bf16[256,1408]{1,0:T(8,128)(2,1)S(1)}, u32[]{:S(2)}, u32[]{:S(2)}) %collective-permute-start.20) | collective-permute-done | bytes 720928 | tf_op jit(solution)/shard_map/ppermute | solution.py:132
  125.8 4.4 %collective-permute-start.15 = (bf16[256,1408]{1,0:T(8,128)(2,1)S(1)}, bf16[256,1408]{1,0:T(8,128)(2,1)S(1)}, u32[]{:S(2)}, u32[]{:S(2)}) collective-permute-start(bf16[256,1408]{1,0:T(8,128)(2,1)S(1)} %fusion.9), channel_id=1, source_target_pairs={{0,8},{4,12},{8,16},{12,20},{1,9},{5,13},{9,17},{13,21},{2,10},{6,... | collective-permute-start | bytes 2162696 | tf_op jit(solution)/shard_map/ppermute | solution.py:132
  142.5 4.2 %collective-permute-done.15 = bf16[256,1408]{1,0:T(8,128)(2,1)S(1)} collective-permute-done((bf16[256,1408]{1,0:T(8,128)(2,1)S(1)}, bf16[256,1408]{1,0:T(8,128)(2,1)S(1)}, u32[]{:S(2)}, u32[]{:S(2)}) %collective-permute-start.15) | collective-permute-done | bytes 720928 | tf_op jit(solution)/shard_map/ppermute | solution.py:132
  149.7 8.0 %collective-permute-done.21 = bf16[256,1408]{1,0:T(8,128)(2,1)S(1)} collective-permute-done((bf16[256,1408]{1,0:T(8,128)(2,1)S(1)}, bf16[256,1408]{1,0:T(8,128)(2,1)S(1)}, u32[]{:S(2)}, u32[]{:S(2)}) %collective-permute-start.21) | collective-permute-done | bytes 720928 | tf_op jit(solution)/shard_map/ppermute | solution.py:132
  162.3 2.5 %fusion.32 = f32[512,256]{0,1:T(8,128)S(1)} fusion(bf16[512,1408]{1,0:T(8,128)(2,1)} %get-tuple-element.11, bf16[2,256,1408]{2,1,0:T(8,128)(2,1)S(1)} %broadcast_select_fusion), kind=kOutput, calls=%fused_computation.79 | convolution fusion | flops 369098752 | bytes 2686976 | tf_op jit(solution)/shard_map/dot_general | solution.py:100
  165.4 7.7 %collective-permute-done.3 = bf16[2,256,1408]{2,1,0:T(8,128)(2,1)S(1)} collective-permute-done((bf16[2,256,1408]{2,1,0:T(8,128)(2,1)}, bf16[2,256,1408]{2,1,0:T(8,128)(2,1)S(1)}, u32[]{:S(2)}, u32[]{:S(2)}) %collective-permute-start.3) | collective-permute-done | bytes 1441824 | tf_op jit(solution)/shard_map/ppermute | solution.py:132
  173.2 2.5 %fusion.28 = f32[512,256]{0,1:T(8,128)S(1)} fusion(bf16[512,1408]{1,0:T(8,128)(2,1)} %get-tuple-element.11, bf16[2,256,1408]{2,1,0:T(8,128)(2,1)S(1)} %broadcast_select_fusion.2), kind=kOutput, calls=%fused_computation.75 | convolution fusion | flops 369098752 | bytes 2686976 | tf_op jit(solution)/shard_map/dot_general | solution.py:100
  177.1 2.5 %copy.22 = bf16[1,2,2,128,1024]{4,3,1,0,2:T(8,128)(2,1)} copy(bf16[1,2,2,128,1024]{3,2,1,4,0:T(2,128)(2,1)S(1)} %stack.53) | data formatting | bytes 2097152 | tf_op jit(solution)/shard_map/stack | solution.py:208
  189.1 3.8 %copy.23 = bf16[1,2,2,128,1024]{4,3,1,0,2:T(8,128)(2,1)} copy(bf16[1,2,2,128,1024]{3,2,1,4,0:T(2,128)(2,1)} %stack.54) | data formatting | bytes 2097152 | tf_op jit(solution)/shard_map/stack | solution.py:208
  195.7 2.9 %collective-permute-start.16 = (bf16[256,1408]{1,0:T(8,128)(2,1)}, bf16[256,1408]{1,0:T(8,128)(2,1)S(1)}, u32[]{:S(2)}, u32[]{:S(2)}) collective-permute-start(bf16[256,1408]{1,0:T(8,128)(2,1)} %get-tuple-element.26), channel_id=1, source_target_pairs={{0,8},{4,12},{8,16},{12,20},{16,24},{20,28},{1,9},{5,13},{9,17},{1... | collective-permute-start | bytes 2162696 | tf_op jit(solution)/shard_map/ppermute | solution.py:132
  208.2 7.2 %collective-permute-done.16 = bf16[256,1408]{1,0:T(8,128)(2,1)S(1)} collective-permute-done((bf16[256,1408]{1,0:T(8,128)(2,1)}, bf16[256,1408]{1,0:T(8,128)(2,1)S(1)}, u32[]{:S(2)}, u32[]{:S(2)}) %collective-permute-start.16) | collective-permute-done | bytes 720928 | tf_op jit(solution)/shard_map/ppermute | solution.py:132
  215.4 7.5 %collective-permute-done.19 = bf16[256,1408]{1,0:T(8,128)(2,1)S(1)} collective-permute-done((bf16[256,1408]{1,0:T(8,128)(2,1)S(1)}, bf16[256,1408]{1,0:T(8,128)(2,1)S(1)}, u32[]{:S(2)}, u32[]{:S(2)}) %collective-permute-start.19) | collective-permute-done | bytes 720928 | tf_op jit(solution)/shard_map/ppermute | solution.py:132
  225.2 5.2 %collective-permute-done.22 = bf16[256,1408]{1,0:T(8,128)(2,1)S(1)} collective-permute-done((bf16[256,1408]{1,0:T(8,128)(2,1)}, bf16[256,1408]{1,0:T(8,128)(2,1)S(1)}, u32[]{:S(2)}, u32[]{:S(2)}) %collective-permute-start.22) | collective-permute-done | bytes 720928 | tf_op jit(solution)/shard_map/ppermute | solution.py:132
  230.4 7.2 %collective-permute-done.25 = bf16[256,1408]{1,0:T(8,128)(2,1)S(1)} collective-permute-done((bf16[256,1408]{1,0:T(8,128)(2,1)S(1)}, bf16[256,1408]{1,0:T(8,128)(2,1)S(1)}, u32[]{:S(2)}, u32[]{:S(2)}) %collective-permute-start.25) | collective-permute-done | bytes 720928 | tf_op jit(solution)/shard_map/ppermute | solution.py:132
  (151 shorter events, 80.2 us)
Async XLA Ops:
  2.2 21.8 %collective-permute-start.11 = (bf16[128,1024]{0,1:T(8,128)(2,1)S(1)}, bf16[128,1024]{0,1:T(8,128)(2,1)S(1)}, u32[]{:S(2)}, u32[]{:S(2)}) collective-permute-start(bf16[128,1024]{0,1:T(8,128)(2,1)S(1)} %bitcast.147), channel_id=1, source_target_pairs={{0,4},{4,0},{8,12},{12,8},{16,20},{20,16},{24,28},{28,24},{1,5},{5... | collective-permute-start | bytes 786440 | tf_op jit(solution)/shard_map/ppermute | solution.py:127
  7.0 53.7 %collective-permute-start = (bf16[2,256,1408]{2,1,0:T(8,128)(2,1)S(1)}, bf16[2,256,1408]{2,1,0:T(8,128)(2,1)}, u32[]{:S(2)}, u32[]{:S(2)}) collective-permute-start(bf16[2,256,1408]{2,1,0:T(8,128)(2,1)S(1)} %shard_map.154), channel_id=1, source_target_pairs={{0,8},{4,12},{8,16},{12,20},{16,24},{20,28},{1,9},{5,13},{9,17},{1... | collective-permute-start | bytes 4325384 | tf_op jit(solution)/shard_map/ppermute | solution.py:132
  12.0 50.5 %collective-permute-start.1 = (bf16[2,256,1408]{2,1,0:T(8,128)(2,1)S(1)}, bf16[2,256,1408]{2,1,0:T(8,128)(2,1)}, u32[]{:S(2)}, u32[]{:S(2)}) collective-permute-start(bf16[2,256,1408]{2,1,0:T(8,128)(2,1)S(1)} %shard_map.154), channel_id=1, source_target_pairs={{8,0},{12,4},{16,8},{20,12},{24,16},{28,20},{9,1},{13,5},{17,9},{2... | collective-permute-start | bytes 4325384 | tf_op jit(solution)/shard_map/ppermute | solution.py:132
  23.4 40.3 %collective-permute-start.7 = (bf16[512,1408]{1,0:T(8,128)(2,1)}, bf16[512,1408]{1,0:T(8,128)(2,1)}, u32[]{:S(2)}, u32[]{:S(2)}) collective-permute-start(bf16[512,1408]{1,0:T(8,128)(2,1)} %get-tuple-element.11), channel_id=1, source_target_pairs={{0,4},{4,0},{8,12},{12,8},{16,20},{20,16},{24,28},{28,24},{1,5},{5... | collective-permute-start | bytes 4325384 | tf_op jit(solution)/shard_map/ppermute | solution.py:127
  24.8 13.1 %collective-permute-start.12 = (bf16[2,1,128,1024]{2,3,0,1:T(8,128)(2,1)}, bf16[2,1,128,1024]{2,3,0,1:T(8,128)(2,1)}, u32[]{:S(2)}, u32[]{:S(2)}) collective-permute-start(bf16[2,1,128,1024]{2,3,0,1:T(8,128)(2,1)} %get-tuple-element.32), channel_id=1, source_target_pairs={{0,2},{1,3},{2,0},{3,1},{4,6},{5,7},{6,4},{7,5},{8,10},{9,11},{10,... | collective-permute-start | bytes 1572872 | tf_op jit(solution)/shard_map/ppermute | solution.py:127
  26.3 21.6 %collective-permute-start.26 = (f32[8,1408]{1,0:T(8,128)S(1)}, f32[8,1408]{1,0:T(8,128)S(1)}, u32[]{:S(2)}, u32[]{:S(2)}) collective-permute-start(f32[8,1408]{1,0:T(8,128)S(1)} %get-tuple-element.12), channel_id=1, source_target_pairs={{0,16},{4,20},{8,24},{12,28},{16,0},{20,4},{24,8},{28,12},{1,17},{... | collective-permute-start | bytes 135176 | tf_op jit(solution)/shard_map/ppermute | solution.py:127
  40.7 25.8 %collective-permute-start.13 = (bf16[2,2,128,1024]{2,3,0,1:T(8,128)(2,1)}, bf16[2,2,128,1024]{2,3,0,1:T(8,128)(2,1)}, u32[]{:S(2)}, u32[]{:S(2)}) collective-permute-start(bf16[2,2,128,1024]{2,3,0,1:T(8,128)(2,1)} %maximum_select_fusion.1), channel_id=1, source_target_pairs={{0,1},{1,0},{2,3},{3,2},{4,5},{5,4},{6,7},{7,6},{8,9},{9,8},{10,11... | collective-permute-start | bytes 3145736 | tf_op jit(solution)/shard_map/ppermute | solution.py:127
  47.9 4.1 %collective-permute-start.27 = (f32[8,1408]{1,0:T(8,128)S(1)}, f32[8,1408]{1,0:T(8,128)S(1)}, u32[]{:S(2)}, u32[]{:S(2)}) collective-permute-start(f32[8,1408]{1,0:T(8,128)S(1)} %add.222), channel_id=1, source_target_pairs={{0,8},{4,12},{8,0},{12,4},{16,24},{20,28},{24,16},{28,20},{1,9},{5... | collective-permute-start | bytes 135176 | tf_op jit(solution)/shard_map/ppermute | solution.py:127
  52.0 5.4 %collective-permute-start.28 = (f32[8,1408]{1,0:T(8,128)S(1)}, f32[8,1408]{1,0:T(8,128)S(1)}, u32[]{:S(2)}, u32[]{:S(2)}) collective-permute-start(f32[8,1408]{1,0:T(8,128)S(1)} %add.223), channel_id=1, source_target_pairs={{0,4},{4,0},{8,12},{12,8},{16,20},{20,16},{24,28},{28,24},{1,5},{5... | collective-permute-start | bytes 135176 | tf_op jit(solution)/shard_map/ppermute | solution.py:127
  58.0 32.1 %collective-permute-start.6 = (bf16[512,1408]{1,0:T(8,128)(2,1)S(1)}, bf16[512,1408]{1,0:T(8,128)(2,1)}, u32[]{:S(2)}, u32[]{:S(2)}) collective-permute-start(bf16[512,1408]{1,0:T(8,128)(2,1)S(1)} %get-tuple-element.10), channel_id=1, source_target_pairs={{0,4},{4,0},{8,12},{12,8},{16,20},{20,16},{24,28},{28,24},{1,5},{5... | collective-permute-start | bytes 4325384 | tf_op jit(solution)/shard_map/ppermute | solution.py:127
  60.7 69.7 %collective-permute-start.4 = (bf16[2,256,1408]{2,1,0:T(8,128)(2,1)}, bf16[2,256,1408]{2,1,0:T(8,128)(2,1)}, u32[]{:S(2)}, u32[]{:S(2)}) collective-permute-start(bf16[2,256,1408]{2,1,0:T(8,128)(2,1)} %collective-permute-done), channel_id=1, source_target_pairs={{8,16},{12,20},{16,24},{20,28},{9,17},{13,21},{17,25},{21,29},{10,... | collective-permute-start | bytes 4325384 | tf_op jit(solution)/shard_map/ppermute | solution.py:132
  62.5 69.9 %collective-permute-start.2 = (bf16[2,256,1408]{2,1,0:T(8,128)(2,1)}, bf16[2,256,1408]{2,1,0:T(8,128)(2,1)}, u32[]{:S(2)}, u32[]{:S(2)}) collective-permute-start(bf16[2,256,1408]{2,1,0:T(8,128)(2,1)} %collective-permute-done.1), channel_id=1, source_target_pairs={{8,0},{12,4},{16,8},{20,12},{9,1},{13,5},{17,9},{21,13},{10,2},{14... | collective-permute-start | bytes 4325384 | tf_op jit(solution)/shard_map/ppermute | solution.py:132
  77.6 12.5 %copy-start.13 = (bf16[1,2,2,128,1024]{4,3,2,1,0:T(8,128)(2,1)S(1)}, bf16[1,2,2,128,1024]{4,3,2,1,0:T(8,128)(2,1)}, u32[]{:S(2)}) copy-start(bf16[1,2,2,128,1024]{4,3,2,1,0:T(8,128)(2,1)} %copy.33) | copy-start | bytes 3145732
  93.3 53.4 %copy-start.9 = (bf16[1024,1408]{1,0:T(8,128)(2,1)}, bf16[1024,1408]{1,0:T(8,128)(2,1)S(1)}, u32[]{:S(2)}) copy-start(bf16[1024,1408]{1,0:T(8,128)(2,1)S(1)} %add_convert_fusion.1) | copy-start | bytes 8650756
  93.5 20.5 %collective-permute-start.14 = (bf16[256,1408]{1,0:T(8,128)(2,1)S(1)}, bf16[256,1408]{1,0:T(8,128)(2,1)S(1)}, u32[]{:S(2)}, u32[]{:S(2)}) collective-permute-start(bf16[256,1408]{1,0:T(8,128)(2,1)S(1)} %get-tuple-element.28), channel_id=1, source_target_pairs={{0,8},{4,12},{1,9},{5,13},{2,10},{6,14},{3,11},{7,15}} | collective-permute-start | bytes 2162696 | tf_op jit(solution)/shard_map/ppermute | solution.py:132
  100.9 56.8 %copy-start.7 = (bf16[1024,1408]{1,0:T(8,128)(2,1)}, bf16[1024,1408]{1,0:T(8,128)(2,1)S(1)}, u32[]{:S(2)}) copy-start(bf16[1024,1408]{1,0:T(8,128)(2,1)S(1)} %add_convert_fusion) | copy-start | bytes 8650756
  101.0 24.8 %collective-permute-start.20 = (bf16[256,1408]{1,0:T(8,128)(2,1)S(1)}, bf16[256,1408]{1,0:T(8,128)(2,1)S(1)}, u32[]{:S(2)}, u32[]{:S(2)}) collective-permute-start(bf16[256,1408]{1,0:T(8,128)(2,1)S(1)} %get-tuple-element.24), channel_id=1, source_target_pairs={{0,8},{4,12},{1,9},{5,13},{2,10},{6,14},{3,11},{7,15}} | collective-permute-start | bytes 2162696 | tf_op jit(solution)/shard_map/ppermute | solution.py:132
  104.5 36.7 %collective-permute-start.17 = (bf16[256,1408]{1,0:T(8,128)(2,1)S(1)}, bf16[256,1408]{1,0:T(8,128)(2,1)S(1)}, u32[]{:S(2)}, u32[]{:S(2)}) collective-permute-start(bf16[256,1408]{1,0:T(8,128)(2,1)S(1)} %get-tuple-element.29), channel_id=1, source_target_pairs={{24,16},{28,20},{25,17},{29,21},{26,18},{30,22},{27,19},{31,23}} | collective-permute-start | bytes 2162696 | tf_op jit(solution)/shard_map/ppermute | solution.py:132
  114.0 35.8 %collective-permute-start.23 = (bf16[256,1408]{1,0:T(8,128)(2,1)S(1)}, bf16[256,1408]{1,0:T(8,128)(2,1)S(1)}, u32[]{:S(2)}, u32[]{:S(2)}) collective-permute-start(bf16[256,1408]{1,0:T(8,128)(2,1)S(1)} %get-tuple-element.25), channel_id=1, source_target_pairs={{24,16},{28,20},{25,17},{29,21},{26,18},{30,22},{27,19},{31,23}} | collective-permute-start | bytes 2162696 | tf_op jit(solution)/shard_map/ppermute | solution.py:132
  125.8 20.9 %collective-permute-start.15 = (bf16[256,1408]{1,0:T(8,128)(2,1)S(1)}, bf16[256,1408]{1,0:T(8,128)(2,1)S(1)}, u32[]{:S(2)}, u32[]{:S(2)}) collective-permute-start(bf16[256,1408]{1,0:T(8,128)(2,1)S(1)} %fusion.9), channel_id=1, source_target_pairs={{0,8},{4,12},{8,16},{12,20},{1,9},{5,13},{9,17},{13,21},{2,10},{6,... | collective-permute-start | bytes 2162696 | tf_op jit(solution)/shard_map/ppermute | solution.py:132
  130.5 27.3 %collective-permute-start.21 = (bf16[256,1408]{1,0:T(8,128)(2,1)S(1)}, bf16[256,1408]{1,0:T(8,128)(2,1)S(1)}, u32[]{:S(2)}, u32[]{:S(2)}) collective-permute-start(bf16[256,1408]{1,0:T(8,128)(2,1)S(1)} %fusion.3), channel_id=1, source_target_pairs={{0,8},{4,12},{8,16},{12,20},{1,9},{5,13},{9,17},{13,21},{2,10},{6,... | collective-permute-start | bytes 2162696 | tf_op jit(solution)/shard_map/ppermute | solution.py:132
  136.5 24.3 %collective-permute-start.5 = (bf16[2,256,1408]{2,1,0:T(8,128)(2,1)}, bf16[2,256,1408]{2,1,0:T(8,128)(2,1)S(1)}, u32[]{:S(2)}, u32[]{:S(2)}) collective-permute-start(bf16[2,256,1408]{2,1,0:T(8,128)(2,1)} %collective-permute-done.4), channel_id=1, source_target_pairs={{16,24},{20,28},{17,25},{21,29},{18,26},{22,30},{19,27},{23,31}} | collective-permute-start | bytes 4325384 | tf_op jit(solution)/shard_map/ppermute | solution.py:132
  141.2 31.8 %collective-permute-start.3 = (bf16[2,256,1408]{2,1,0:T(8,128)(2,1)}, bf16[2,256,1408]{2,1,0:T(8,128)(2,1)S(1)}, u32[]{:S(2)}, u32[]{:S(2)}) collective-permute-start(bf16[2,256,1408]{2,1,0:T(8,128)(2,1)} %collective-permute-done.2), channel_id=1, source_target_pairs={{8,0},{12,4},{9,1},{13,5},{10,2},{14,6},{11,3},{15,7}} | collective-permute-start | bytes 4325384 | tf_op jit(solution)/shard_map/ppermute | solution.py:132
  148.2 52.4 %collective-permute-start.18 = (bf16[256,1408]{1,0:T(8,128)(2,1)}, bf16[256,1408]{1,0:T(8,128)(2,1)}, u32[]{:S(2)}, u32[]{:S(2)}) collective-permute-start(bf16[256,1408]{1,0:T(8,128)(2,1)} %get-tuple-element.27), channel_id=1, source_target_pairs={{16,8},{20,12},{24,16},{28,20},{17,9},{21,13},{25,17},{29,21},{18,... | collective-permute-start | bytes 2162696 | tf_op jit(solution)/shard_map/ppermute | solution.py:132
  159.2 44.1 %collective-permute-start.24 = (bf16[256,1408]{1,0:T(8,128)(2,1)}, bf16[256,1408]{1,0:T(8,128)(2,1)}, u32[]{:S(2)}, u32[]{:S(2)}) collective-permute-start(bf16[256,1408]{1,0:T(8,128)(2,1)} %get-tuple-element.23), channel_id=1, source_target_pairs={{16,8},{20,12},{24,16},{28,20},{17,9},{21,13},{25,17},{29,21},{18,... | collective-permute-start | bytes 2162696 | tf_op jit(solution)/shard_map/ppermute | solution.py:132
  194.3 11.8 %collective-permute-start.8 = (bf16[2,2,128,1024]{3,2,1,0:T(8,128)(2,1)S(1)}, bf16[2,2,128,1024]{3,2,1,0:T(8,128)(2,1)S(1)}, u32[]{:S(2)}, u32[]{:S(2)}) collective-permute-start(bf16[2,2,128,1024]{3,2,1,0:T(8,128)(2,1)S(1)} %fusion.22), channel_id=1, source_target_pairs={{0,1},{1,0},{2,3},{3,2},{4,5},{5,4},{6,7},{7,6},{8,9},{9,8},{10,11... | collective-permute-start | bytes 3145736 | tf_op jit(solution)/shard_map/ppermute | solution.py:127
  195.7 19.7 %collective-permute-start.16 = (bf16[256,1408]{1,0:T(8,128)(2,1)}, bf16[256,1408]{1,0:T(8,128)(2,1)S(1)}, u32[]{:S(2)}, u32[]{:S(2)}) collective-permute-start(bf16[256,1408]{1,0:T(8,128)(2,1)} %get-tuple-element.26), channel_id=1, source_target_pairs={{0,8},{4,12},{8,16},{12,20},{16,24},{20,28},{1,9},{5,13},{9,17},{1... | collective-permute-start | bytes 2162696 | tf_op jit(solution)/shard_map/ppermute | solution.py:132
  198.6 31.7 %collective-permute-start.22 = (bf16[256,1408]{1,0:T(8,128)(2,1)}, bf16[256,1408]{1,0:T(8,128)(2,1)S(1)}, u32[]{:S(2)}, u32[]{:S(2)}) collective-permute-start(bf16[256,1408]{1,0:T(8,128)(2,1)} %get-tuple-element.22), channel_id=1, source_target_pairs={{0,8},{4,12},{8,16},{12,20},{16,24},{20,28},{1,9},{5,13},{9,17},{1... | collective-permute-start | bytes 2162696 | tf_op jit(solution)/shard_map/ppermute | solution.py:132
  201.9 21.0 %collective-permute-start.19 = (bf16[256,1408]{1,0:T(8,128)(2,1)S(1)}, bf16[256,1408]{1,0:T(8,128)(2,1)S(1)}, u32[]{:S(2)}, u32[]{:S(2)}) collective-permute-start(bf16[256,1408]{1,0:T(8,128)(2,1)S(1)} %fusion.8), channel_id=1, source_target_pairs={{8,0},{12,4},{16,8},{20,12},{24,16},{28,20},{9,1},{13,5},{17,9},{2... | collective-permute-start | bytes 2162696 | tf_op jit(solution)/shard_map/ppermute | solution.py:132
  204.7 33.0 %collective-permute-start.25 = (bf16[256,1408]{1,0:T(8,128)(2,1)S(1)}, bf16[256,1408]{1,0:T(8,128)(2,1)S(1)}, u32[]{:S(2)}, u32[]{:S(2)}) collective-permute-start(bf16[256,1408]{1,0:T(8,128)(2,1)S(1)} %fusion.2), channel_id=1, source_target_pairs={{8,0},{12,4},{16,8},{20,12},{24,16},{28,20},{9,1},{13,5},{17,9},{2... | collective-permute-start | bytes 2162696 | tf_op jit(solution)/shard_map/ppermute | solution.py:132
  206.7 17.6 %collective-permute-start.9 = (bf16[2,1,128,1024]{3,2,1,0:T(8,128)(2,1)S(1)}, bf16[2,1,128,1024]{3,2,1,0:T(8,128)(2,1)S(1)}, u32[]{:S(2)}, u32[]{:S(2)}) collective-permute-start(bf16[2,1,128,1024]{3,2,1,0:T(8,128)(2,1)S(1)} %constant_dynamic-slice_fusion.2), channel_id=1, source_target_pairs={{0,2},{1,3},{2,0},{3,1},{4,6},{5,7},{6,4},{7,5},{8,10},{9,11},{10,... | collective-permute-start | bytes 1572872 | tf_op jit(solution)/shard_map/ppermute | solution.py:127
  224.6 14.8 %collective-permute-start.10 = (bf16[128,1024]{1,0:T(8,128)(2,1)S(1)}, bf16[128,1024]{1,0:T(8,128)(2,1)S(1)}, u32[]{:S(2)}, u32[]{:S(2)}) collective-permute-start(bf16[128,1024]{1,0:T(8,128)(2,1)S(1)} %get-tuple-element.37), channel_id=1, source_target_pairs={{0,4},{4,0},{8,12},{12,8},{16,20},{20,16},{24,28},{28,24},{1,5},{5... | collective-permute-start | bytes 786440 | tf_op jit(solution)/shard_map/ppermute | solution.py:127
  (23 other events, 110.0 us)
